TPU v7x, 128 devices: a whole 4x4x4 slice. The times are simulated.
128 devices in a mesh: sp: 16 (over z, y), tp: 8 (over x, core).
Axes of the slice: x: 4, y: 4, z: 4, core: 2. Of those that a mesh axis runs over, the one named last changes fastest.
Arguments:
- tokens: bfloat16 [12288, 2048], P('sp', 'tp'), may hold values from -6 to 6
- norm_gain: float32 [2048], replicated, may hold values from 0.1 to 1.9
- w_query: bfloat16 [2048, 2048], P(None, 'tp'), may hold values from -4 to 4
- w_key: bfloat16 [2048, 2048], P(None, 'tp'), may hold values from -4 to 4
- w_value: bfloat16 [2048, 2048], P(None, 'tp'), may hold values from -0.125 to 0.125
- w_outer: bfloat16 [2048, 2048], P(None, 'tp'), may hold values from -0.125 to 0.125
- w_inner: bfloat16 [2048, 2048], P(None, 'tp'), may hold values from -0.125 to 0.125
- w_signal: bfloat16 [2048, 2048], P(None, 'tp'), may hold values from -0.125 to 0.125
- conv_taps: bfloat16 [3, 2048], P(None, 'tp'), may hold values from -3.5 to 3.5
- lambdas: float32 [8], P('tp'), may hold values from 0.3 to 0.8
- head_gain: float32 [256], replicated, may hold values from 0.1 to 1.9
- attend_proj: bfloat16 [2048, 2048], P('tp'), may hold values from -0.125 to 0.125
- convolve_proj: bfloat16 [2048, 2048], P('tp'), may hold values from -0.125 to 0.125
Outputs:
- mixed: bfloat16 [12288, 2048], P(('sp', 'tp'))
- row_lse: float32 [12288, 16], P('sp', 'tp')
All inputs are finite; a program needn't handle non-finite values.
Results may differ from a plain program's by a relative error of at most 0.015.
Values may be sent and summed in bfloat16 or wider, within the bound.
A program may use at most 128 MiB of HBM per device.

v0:
```python
import jax
import jax.numpy as jnp
from jax import lax
from jax.sharding import PartitionSpec as P

ROPE_BASE = 500000.0
NORM_EPS = 1e-05
HEAD_KEEP = 0.8
MASKED = -1e30


def passed_along(value, axis, steps):
    count = lax.axis_size(axis)
    initial, last = (max(0, -steps), min(count, count - steps))
    return lax.ppermute(value, axis, [(source, source + steps) for source in range(initial, last)])


def rotate(values_in, positions):
    half_width = values_in.shape[-1] // 2
    inverse = ROPE_BASE ** (-jnp.arange(half_width, dtype=jnp.float32) * 2.0 / values_in.shape[-1])
    angles = positions.astype(jnp.float32)[:, None] * inverse[None, :]
    cosine = jnp.cos(angles)[:, None, :]
    sine_part = jnp.sin(angles)[:, None, :]
    first_half = values_in[..., :half_width]
    second_half = values_in[..., half_width:]
    return jnp.concatenate(
        [
            first_half * cosine - second_half * sine_part,
            second_half * cosine + first_half * sine_part,
        ],
        axis=-1,
    )


def absorb(state, queries, positions, key_block, value_block, first_key):
    running_max, weight_sum, weighted = state
    head_count = weighted.shape[0]
    block_rows = key_block.shape[0]
    scores = jnp.einsum("qgd,kgd->gqk", queries, key_block, preferred_element_type=jnp.float32)
    scores = scores * queries.shape[-1] ** (-0.5)
    key_places = first_key + jnp.arange(block_rows, dtype=jnp.int32)
    allowed = key_places[None, :] <= positions[:, None]
    scores = jnp.where(allowed[None], scores, MASKED)
    scores = scores.reshape(head_count, 2, positions.shape[0], block_rows)
    raised = jnp.maximum(running_max, jnp.max(scores, axis=3))
    factor = jnp.exp(running_max - raised)
    lifted = jnp.exp(scores - raised[..., None])
    weight_sum = factor * weight_sum + jnp.sum(lifted, axis=3)
    values_here = value_block.reshape(block_rows, head_count, -1)
    weighted = factor[..., None] * weighted + jnp.einsum(
        "hjqk,khe->hjqe",
        lifted.astype(jnp.bfloat16),
        values_here,
        preferred_element_type=jnp.float32,
    )
    return (raised, weight_sum, weighted)


def empty_state(head_count, rows, head_width):
    return (
        jnp.full((head_count, 2, rows), MASKED, jnp.float32),
        jnp.zeros((head_count, 2, rows), jnp.float32),
        jnp.zeros((head_count, 2, rows, 2 * head_width), jnp.float32),
    )


def finish(state, lambdas, head_gain):
    running_max, weight_sum, weighted = state
    head_count = weighted.shape[0]
    rows = weighted.shape[2]
    normalized = weighted / weight_sum[..., None]
    difference = normalized[:, 0] - lambdas[:, None, None] * normalized[:, 1]
    scale_back = lax.rsqrt(jnp.mean(difference * difference, axis=2, keepdims=True) + NORM_EPS)
    attended = (difference * scale_back * head_gain[None, None, :] * HEAD_KEEP).astype(jnp.bfloat16)
    attended = jnp.transpose(attended, (1, 0, 2)).reshape(rows, head_count * weighted.shape[3])
    row_lse = jnp.transpose(running_max + jnp.log(weight_sum), (2, 0, 1)).reshape(
        rows, 2 * head_count
    )
    return (attended, row_lse)


def make_fold(groups, row_count, carry, pieces):
    key_piece, value_piece = pieces
    block_rows = min(key_piece.shape[0], row_count)
    shard_count = key_piece.shape[0] // block_rows

    def one_shard(inner_states, shard_index):
        first_key = shard_index * block_rows
        key_block = lax.dynamic_slice_in_dim(key_piece, shard_index * block_rows, block_rows, 0)
        value_block = lax.dynamic_slice_in_dim(value_piece, shard_index * block_rows, block_rows, 0)
        updated_states = []
        for given_state, group in zip(inner_states, groups):
            group_queries, group_places, group_last = group

            def take_block(given):
                return absorb(given, group_queries, group_places, key_block, value_block, first_key)

            def leave_block(given):
                return given

            updated_states.append(
                lax.cond(first_key < group_last, take_block, leave_block, given_state)
            )
        return (tuple(updated_states), None)

    carry, _ = lax.scan(one_shard, carry, jnp.arange(shard_count, dtype=jnp.int32))
    return carry


def per_device(
    tokens,
    norm_gain,
    w_query,
    w_key,
    w_value,
    w_outer,
    w_inner,
    w_signal,
    conv_taps,
    lambdas,
    head_gain,
    attend_proj,
    convolve_proj,
):
    row_count = tokens.shape[0]
    model_width = norm_gain.shape[0]
    head_count = lambdas.shape[0]
    head_width = w_query.shape[1] // (2 * head_count)
    projections = (w_query, w_key, w_value, w_outer, w_inner, w_signal)
    widened = lax.all_gather(tokens, "tp", axis=1, tiled=True).astype(jnp.float32)
    scaled = (widened * norm_gain[None, :]).astype(jnp.bfloat16)
    squares = jnp.sum(widened * widened, axis=1)
    sums = tuple(
        (jnp.dot(scaled, weight, preferred_element_type=jnp.float32) for weight in projections)
    )
    folded = (squares,) + sums
    inv_rms = lax.rsqrt(folded[0] / model_width + NORM_EPS)[:, None]
    offset = lax.axis_index("sp") * row_count
    positions = offset + jnp.arange(row_count, dtype=jnp.int32)
    queries = rotate(
        (inv_rms * folded[1]).reshape(row_count, 2 * head_count, head_width), positions
    ).astype(jnp.bfloat16)
    key_rows = rotate(
        (inv_rms * folded[2]).reshape(row_count, 2 * head_count, head_width), positions
    ).astype(jnp.bfloat16)
    value_rows = (inv_rms * folded[3]).astype(jnp.bfloat16)
    outer_gate = inv_rms * folded[4]
    product = inv_rms * folded[5] * (inv_rms * folded[6])
    groups = ((queries, positions, offset + row_count),)
    states = make_fold(
        groups,
        row_count,
        (empty_state(head_count, row_count, head_width),),
        (
            lax.all_gather(key_rows, "sp", axis=0, tiled=True),
            lax.all_gather(value_rows, "sp", axis=0, tiled=True),
        ),
    )
    attended, row_lse = finish(states[0], lambdas, head_gain)
    border = passed_along(product[row_count - 2 :], "sp", 1)
    padded = jnp.concatenate([border, product], axis=0)
    tap_values = conv_taps.astype(jnp.float32)
    smoothed = (
        tap_values[0] * padded[:-2] + tap_values[1] * padded[1:-1] + tap_values[2] * padded[2:]
    )
    convolved = (outer_gate * smoothed).astype(jnp.bfloat16)
    mixed = lax.psum_scatter(
        (
            jnp.dot(attended, attend_proj, preferred_element_type=jnp.float32)
            + jnp.dot(convolved, convolve_proj, preferred_element_type=jnp.float32)
        ).astype(jnp.bfloat16),
        "tp",
        scatter_dimension=0,
        tiled=True,
    )
    return (mixed, row_lse)


def solution(mesh):
    return jax.shard_map(
        per_device,
        mesh=mesh,
        in_specs=(
            P("sp", "tp"),
            P(),
            P(None, "tp"),
            P(None, "tp"),
            P(None, "tp"),
            P(None, "tp"),
            P(None, "tp"),
            P(None, "tp"),
            P(None, "tp"),
            P("tp"),
            P(),
            P("tp", None),
            P("tp", None),
        ),
        out_specs=(P(("sp", "tp"), None), P("sp", "tp")),
        check_vma=False,
    )
```

profile of v0, /device:TPU:97, one launch (start us, length us, event | category | flops | bytes accessed | tf_op | source)
XLA Modules:
  0.0 350.7 jit_solution(7850636418665392212)
XLA Ops:
  8.0 34.5 %all-gather.4.cloned.1.call-done = bf16[768,2048]{1,0:T(8,128)(2,1)} async-done(((bf16[768,256]{1,0:T(8,128)(2,1)}), bf16[768,2048]{1,0:T(8,128)(2,1)}) %all-gather.4.cloned.1.call-update) | async-done | bytes 3145744 | tf_op jit(solution)/shard_map/all_gather | solution.py:130
  45.1 4.0 %fusion.31 = bf16[768,256]{0,1:T(8,128)(2,1)} fusion(bf16[2048,256]{1,0:T(8,128)(2,1)} %param.21, bf16[768,2048]{1,0:T(8,128)(2,1)} %all-gather.4.cloned.1.call-done, f32[2048]{0:T(1024)} %param.18, f32[768]{0:T(1024)S(1)} %add_rsqrt_fusion.1), kind=kOutput, calls=%fused_computation.39 | convolution fusion | flops 810418176 | bytes 4598784 | tf_op jit(solution)/shard_map/dot_general | solution.py:134
  67.4 3.5 convolution_multiply_fusion.1
  73.0 3.3 collective-permute-start
  77.3 33.4 %all-gather.8.cloned.1.call-done = bf16[12288,256]{0,1:T(8,128)(2,1)} async-done(((bf16[768,256]{0,1:T(8,128)(2,1)}), bf16[12288,256]{0,1:T(8,128)(2,1)}) %all-gather.8.cloned.1.call-update) | async-done | bytes 6291472 | tf_op jit(solution)/shard_map/all_gather | solution.py:156
  110.6 8.6 %copy.21 = bf16[12288,256]{1,0:T(8,128)(2,1)} copy(bf16[12288,256]{0,1:T(8,128)(2,1)} %all-gather.8.cloned.1.call-done) | data formatting | bytes 12582912
  119.2 54.6 %all-gather.6.cloned.1.call-done = bf16[12288,2,128]{2,0,1:T(8,128)(2,1)} async-done(((bf16[768,2,128]{2,0,1:T(8,128)(2,1)}), bf16[12288,2,128]{2,0,1:T(8,128)(2,1)}) %all-gather.6.cloned.1.call-update) | async-done | bytes 6291472 | tf_op jit(solution)/shard_map/all_gather | solution.py:155
  173.9 105.6 %while.15 = (s32[]{:T(128)}, f32[1,2,768]{2,1,0:T(2,128)S(1)}, f32[1,2,768]{2,1,0:T(2,128)S(1)}, f32[1,2,768,256]{3,2,1,0:T(8,128)S(1)}, s32[16]{0:T(128)S(1)}, ...) while((s32[]{:T(128)}, f32[1,2,768]{2,1,0:T(2,128)S(1)}, ...), condition=%wide.region_6.7_spmd.clone, body=%wide.region_1.6_spmd.clone.sunk | while | flops 920328192 | bytes 20957516 | solution.py:106
  175.2 6.5 %conditional.3 = ((f32[1,2,768]{2,1,0:T(2,128)S(1)}, f32[1,2,768]{2,1,0:T(2,128)S(1)}, f32[1,2,768,256]{3,2,1,0:T(8,128)S(1)})) conditional(s32[]{:T(128)} %convert_element_type.96, (f32[1,2,768]{2,1,0:T(2,128)S(1)}, f32[1,2,768]{2,1,0:T(2,128)S(1)}, f32[1,2,768,256]{3,2,1,0:T(8,128)S(1)}) %tuple.58, (s32[]{:T(128)}, s32[]{:T(128)}, ...), branch_computations={%region_2.2_spmd, %region_3.5_spmd} | conditional | flops 920328192 | bytes 20954194 | solution.py:102
  183.0 6.5 %conditional.3 = ((f32[1,2,768]{2,1,0:T(2,128)S(1)}, f32[1,2,768]{2,1,0:T(2,128)S(1)}, f32[1,2,768,256]{3,2,1,0:T(8,128)S(1)})) conditional(s32[]{:T(128)} %convert_element_type.96, (f32[1,2,768]{2,1,0:T(2,128)S(1)}, f32[1,2,768]{2,1,0:T(2,128)S(1)}, f32[1,2,768,256]{3,2,1,0:T(8,128)S(1)}) %tuple.58, (s32[]{:T(128)}, s32[]{:T(128)}, ...), branch_computations={%region_2.2_spmd, %region_3.5_spmd} | conditional | flops 920328192 | bytes 20954194 | solution.py:102
  190.8 6.5 %conditional.3 = ((f32[1,2,768]{2,1,0:T(2,128)S(1)}, f32[1,2,768]{2,1,0:T(2,128)S(1)}, f32[1,2,768,256]{3,2,1,0:T(8,128)S(1)})) conditional(s32[]{:T(128)} %convert_element_type.96, (f32[1,2,768]{2,1,0:T(2,128)S(1)}, f32[1,2,768]{2,1,0:T(2,128)S(1)}, f32[1,2,768,256]{3,2,1,0:T(8,128)S(1)}) %tuple.58, (s32[]{:T(128)}, s32[]{:T(128)}, ...), branch_computations={%region_2.2_spmd, %region_3.5_spmd} | conditional | flops 920328192 | bytes 20954194 | solution.py:102
  198.7 6.5 %conditional.3 = ((f32[1,2,768]{2,1,0:T(2,128)S(1)}, f32[1,2,768]{2,1,0:T(2,128)S(1)}, f32[1,2,768,256]{3,2,1,0:T(8,128)S(1)})) conditional(s32[]{:T(128)} %convert_element_type.96, (f32[1,2,768]{2,1,0:T(2,128)S(1)}, f32[1,2,768]{2,1,0:T(2,128)S(1)}, f32[1,2,768,256]{3,2,1,0:T(8,128)S(1)}) %tuple.58, (s32[]{:T(128)}, s32[]{:T(128)}, ...), branch_computations={%region_2.2_spmd, %region_3.5_spmd} | conditional | flops 920328192 | bytes 20954194 | solution.py:102
  206.5 6.5 %conditional.3 = ((f32[1,2,768]{2,1,0:T(2,128)S(1)}, f32[1,2,768]{2,1,0:T(2,128)S(1)}, f32[1,2,768,256]{3,2,1,0:T(8,128)S(1)})) conditional(s32[]{:T(128)} %convert_element_type.96, (f32[1,2,768]{2,1,0:T(2,128)S(1)}, f32[1,2,768]{2,1,0:T(2,128)S(1)}, f32[1,2,768,256]{3,2,1,0:T(8,128)S(1)}) %tuple.58, (s32[]{:T(128)}, s32[]{:T(128)}, ...), branch_computations={%region_2.2_spmd, %region_3.5_spmd} | conditional | flops 920328192 | bytes 20954194 | solution.py:102
  214.3 6.5 %conditional.3 = ((f32[1,2,768]{2,1,0:T(2,128)S(1)}, f32[1,2,768]{2,1,0:T(2,128)S(1)}, f32[1,2,768,256]{3,2,1,0:T(8,128)S(1)})) conditional(s32[]{:T(128)} %convert_element_type.96, (f32[1,2,768]{2,1,0:T(2,128)S(1)}, f32[1,2,768]{2,1,0:T(2,128)S(1)}, f32[1,2,768,256]{3,2,1,0:T(8,128)S(1)}) %tuple.58, (s32[]{:T(128)}, s32[]{:T(128)}, ...), branch_computations={%region_2.2_spmd, %region_3.5_spmd} | conditional | flops 920328192 | bytes 20954194 | solution.py:102
  222.1 6.5 %conditional.3 = ((f32[1,2,768]{2,1,0:T(2,128)S(1)}, f32[1,2,768]{2,1,0:T(2,128)S(1)}, f32[1,2,768,256]{3,2,1,0:T(8,128)S(1)})) conditional(s32[]{:T(128)} %convert_element_type.96, (f32[1,2,768]{2,1,0:T(2,128)S(1)}, f32[1,2,768]{2,1,0:T(2,128)S(1)}, f32[1,2,768,256]{3,2,1,0:T(8,128)S(1)}) %tuple.58, (s32[]{:T(128)}, s32[]{:T(128)}, ...), branch_computations={%region_2.2_spmd, %region_3.5_spmd} | conditional | flops 920328192 | bytes 20954194 | solution.py:102
  229.9 6.5 %conditional.3 = ((f32[1,2,768]{2,1,0:T(2,128)S(1)}, f32[1,2,768]{2,1,0:T(2,128)S(1)}, f32[1,2,768,256]{3,2,1,0:T(8,128)S(1)})) conditional(s32[]{:T(128)} %convert_element_type.96, (f32[1,2,768]{2,1,0:T(2,128)S(1)}, f32[1,2,768]{2,1,0:T(2,128)S(1)}, f32[1,2,768,256]{3,2,1,0:T(8,128)S(1)}) %tuple.58, (s32[]{:T(128)}, s32[]{:T(128)}, ...), branch_computations={%region_2.2_spmd, %region_3.5_spmd} | conditional | flops 920328192 | bytes 20954194 | solution.py:102
  237.8 6.5 %conditional.3 = ((f32[1,2,768]{2,1,0:T(2,128)S(1)}, f32[1,2,768]{2,1,0:T(2,128)S(1)}, f32[1,2,768,256]{3,2,1,0:T(8,128)S(1)})) conditional(s32[]{:T(128)} %convert_element_type.96, (f32[1,2,768]{2,1,0:T(2,128)S(1)}, f32[1,2,768]{2,1,0:T(2,128)S(1)}, f32[1,2,768,256]{3,2,1,0:T(8,128)S(1)}) %tuple.58, (s32[]{:T(128)}, s32[]{:T(128)}, ...), branch_computations={%region_2.2_spmd, %region_3.5_spmd} | conditional | flops 920328192 | bytes 20954194 | solution.py:102
  245.6 6.5 %conditional.3 = ((f32[1,2,768]{2,1,0:T(2,128)S(1)}, f32[1,2,768]{2,1,0:T(2,128)S(1)}, f32[1,2,768,256]{3,2,1,0:T(8,128)S(1)})) conditional(s32[]{:T(128)} %convert_element_type.96, (f32[1,2,768]{2,1,0:T(2,128)S(1)}, f32[1,2,768]{2,1,0:T(2,128)S(1)}, f32[1,2,768,256]{3,2,1,0:T(8,128)S(1)}) %tuple.58, (s32[]{:T(128)}, s32[]{:T(128)}, ...), branch_computations={%region_2.2_spmd, %region_3.5_spmd} | conditional | flops 920328192 | bytes 20954194 | solution.py:102
  253.4 6.5 %conditional.3 = ((f32[1,2,768]{2,1,0:T(2,128)S(1)}, f32[1,2,768]{2,1,0:T(2,128)S(1)}, f32[1,2,768,256]{3,2,1,0:T(8,128)S(1)})) conditional(s32[]{:T(128)} %convert_element_type.96, (f32[1,2,768]{2,1,0:T(2,128)S(1)}, f32[1,2,768]{2,1,0:T(2,128)S(1)}, f32[1,2,768,256]{3,2,1,0:T(8,128)S(1)}) %tuple.58, (s32[]{:T(128)}, s32[]{:T(128)}, ...), branch_computations={%region_2.2_spmd, %region_3.5_spmd} | conditional | flops 920328192 | bytes 20954194 | solution.py:102
  261.2 6.5 %conditional.3 = ((f32[1,2,768]{2,1,0:T(2,128)S(1)}, f32[1,2,768]{2,1,0:T(2,128)S(1)}, f32[1,2,768,256]{3,2,1,0:T(8,128)S(1)})) conditional(s32[]{:T(128)} %convert_element_type.96, (f32[1,2,768]{2,1,0:T(2,128)S(1)}, f32[1,2,768]{2,1,0:T(2,128)S(1)}, f32[1,2,768,256]{3,2,1,0:T(8,128)S(1)}) %tuple.58, (s32[]{:T(128)}, s32[]{:T(128)}, ...), branch_computations={%region_2.2_spmd, %region_3.5_spmd} | conditional | flops 920328192 | bytes 20954194 | solution.py:102
  269.1 6.5 %conditional.3 = ((f32[1,2,768]{2,1,0:T(2,128)S(1)}, f32[1,2,768]{2,1,0:T(2,128)S(1)}, f32[1,2,768,256]{3,2,1,0:T(8,128)S(1)})) conditional(s32[]{:T(128)} %convert_element_type.96, (f32[1,2,768]{2,1,0:T(2,128)S(1)}, f32[1,2,768]{2,1,0:T(2,128)S(1)}, f32[1,2,768,256]{3,2,1,0:T(8,128)S(1)}) %tuple.58, (s32[]{:T(128)}, s32[]{:T(128)}, ...), branch_computations={%region_2.2_spmd, %region_3.5_spmd} | conditional | flops 920328192 | bytes 20954194 | solution.py:102
  280.2 3.7 %fusion.45 = f32[768,2048]{1,0:T(8,128)} fusion(bf16[256,2048]{1,0:T(8,128)(2,1)S(1)} %copy-done, f32[256]{0:T(256)S(1)} %copy-done.9, f32[768]{0:T(1024)S(1)} %add_rsqrt_fusion, f32[1,2,768,256]{3,2,1,0:T(8,128)S(1)} %broadcast_divide_fusion, f32[]{:T(128)} %bitcast.56), kind=kOutput, calls=%fused_computation.64 | convolution fusion | flops 806486016 | bytes 8916996 | tf_op jit(solution)/shard_map/dot_general | solution.py:169
  283.9 8.4 %add_convert_fusion = bf16[768,2048]{1,0:T(8,128)(2,1)} fusion(f32[768,2048]{1,0:T(8,128)} %fusion.45, bf16[256,2048]{1,0:T(8,128)(2,1)S(1)} %copy-done.6, f32[2,256]{0,1:T(8,128)S(1)} %collective-permute-done, f32[768,256]{0,1:T(8,128)S(1)} %copy-done.5, bf16[2048,256]{1,0:T(8,128)(2,1)} %param.22, bf16[768,2048]{1,0:T(8,128)(2,1)} %all-gather.4.cloned.1.call-done, ...), kind=kOutput, calls=%fused_computation.31 | convolution fusion | flops 1620443136 | bytes 15482880 | tf_op jit(solution)/shard_map/dot_general | solution.py:170
  292.9 51.2 %reduce-scatter.2.cloned.1.call-done = bf16[96,2048]{1,0:T(8,128)(2,1)} async-done(((bf16[768,2048]{1,0:T(8,128)(2,1)}), bf16[96,2048]{1,0:T(8,128)(2,1)}) %reduce-scatter.2.cloned.1.call-update) | async-done | bytes 393232 | tf_op jit(solution)/shard_map/reduce_scatter | solution.py:167
  (199 shorter events, 119.0 us)
Async XLA Ops:
  7.2 272.9 %copy-start = (bf16[256,2048]{1,0:T(8,128)(2,1)S(1)}, bf16[256,2048]{1,0:T(8,128)(2,1)}, u32[]{:S(2)}) copy-start(bf16[256,2048]{1,0:T(8,128)(2,1)} %param.28) | copy-start | bytes 3145732
  7.2 35.3 %all-gather.4.cloned.1.call-start = ((), (), s32[]{:S(2)}) async-start(), calls=%async_computation.1 | async-start | bytes 3538944 | tf_op jit(solution)/shard_map/all_gather | solution.py:130
  7.9 43.7 %copy-start.7 = (f32[2048]{0:T(1024)S(1)}, f32[2048]{0:T(1024)}, u32[]{:S(2)}) copy-start(f32[2048]{0:T(1024)} %param.18) | copy-start | bytes 24580
  7.9 43.7 %copy-start.10 = (bf16[2048,256]{1,0:T(8,128)(2,1)S(1)}, bf16[2048,256]{1,0:T(8,128)(2,1)}, u32[]{:S(2)}) copy-start(bf16[2048,256]{1,0:T(8,128)(2,1)} %param.20) | copy-start | bytes 3145732
  7.9 102.7 %all-gather.8.cloned.1.call-start = ((), (), s32[]{:S(2)}) async-start(), calls=%async_computation.3 | async-start | bytes 6684672 | tf_op jit(solution)/shard_map/all_gather | solution.py:156
  49.1 124.7 %all-gather.6.cloned.1.call-start = ((), (), s32[]{:S(2)}) async-start(), calls=%async_computation.2 | async-start | bytes 6684672 | tf_op jit(solution)/shard_map/all_gather | solution.py:155
  59.3 8.0 %copy-start.8 = (bf16[3,256]{1,0:T(4,128)(2,1)S(1)}, bf16[3,256]{1,0:T(4,128)(2,1)}, u32[]{:S(2)}) copy-start(bf16[3,256]{1,0:T(4,128)(2,1)} %param.25) | copy-start | bytes 4612
  65.5 5.3 %copy-start.11 = (bf16[2048,256]{1,0:T(8,128)(2,1)S(1)}, bf16[2048,256]{1,0:T(8,128)(2,1)}, u32[]{:S(2)}) copy-start(bf16[2048,256]{1,0:T(8,128)(2,1)} %param.24) | copy-start | bytes 3145732
  66.5 277.6 %reduce-scatter.2.cloned.1.call-start = ((), (), s32[]{:S(2)}) async-start(), calls=%async_computation.4 | async-start | bytes 3538944 | tf_op jit(solution)/shard_map/reduce_scatter | solution.py:167
  66.5 4.3 %copy-start.1 = (bf16[768,2048]{1,0:T(8,128)(2,1)S(1)}, bf16[768,2048]{1,0:T(8,128)(2,1)}, u32[]{:S(2)}) copy-start(bf16[768,2048]{1,0:T(8,128)(2,1)} %all-gather.4.cloned.1.call-done) | copy-start | bytes 9437188
  70.9 5.4 %copy-start.2 = (bf16[768,2,64]{2,0,1:T(8,128)(2,1)S(1)}, bf16[768,2,64]{2,0,1:T(8,128)(2,1)}, u32[]{:S(2)}) copy-start(bf16[768,2,64]{2,0,1:T(8,128)(2,1)} %get-tuple-element.231) | copy-start | bytes 589828
  70.9 5.4 %copy-start.3 = (bf16[768,2,64]{2,0,1:T(8,128)(2,1)S(1)}, bf16[768,2,64]{2,0,1:T(8,128)(2,1)}, u32[]{:S(2)}) copy-start(bf16[768,2,64]{2,0,1:T(8,128)(2,1)} %get-tuple-element.232) | copy-start | bytes 589828
  72.0 0.9 copy-start.4
  73.0 210.9 %collective-permute-start = (f32[2,256]{0,1:T(8,128)S(1)}, f32[2,256]{0,1:T(8,128)S(1)}, u32[]{:S(2)}, u32[]{:S(2)}) collective-permute-start(f32[2,256]{0,1:T(8,128)S(1)} %slice.55), channel_id=1, source_target_pairs={{0,8},{8,16},{16,24},{24,32},{32,40},{40,48},{48,56},{56,64},{64,7... | collective-permute-start | bytes 6152 | tf_op jit(solution)/shard_map/ppermute | solution.py:15
  279.5 0.7 copy-start.9
  280.2 3.7 %copy-start.5 = (f32[768,256]{0,1:T(8,128)S(1)}, f32[768,256]{0,1:T(8,128)}, u32[]{:S(2)}) copy-start(f32[768,256]{0,1:T(8,128)} %copy-done.4) | copy-start | bytes 2359300
  280.2 3.7 %copy-start.6 = (bf16[256,2048]{1,0:T(8,128)(2,1)S(1)}, bf16[256,2048]{1,0:T(8,128)(2,1)}, u32[]{:S(2)}) copy-start(bf16[256,2048]{1,0:T(8,128)(2,1)} %param.29) | copy-start | bytes 3145732
Sparse Core Ops, SparseCore 0:
  9.7 32.7 all-gather.3
  49.2 61.3 all-gather.7
  112.8 60.9 all-gather.5
  292.4 51.6 reduce-scatter.1
where the time goes:
time: 356 us; the launch traced here: 351 us
  waiting for transfers between devices  174 us (49%)
  matrix products  90.9 us (26%)
  other arithmetic  30.5 us (9%)
  local copies, waits for them, and re-layouts  24.8 us (7%)
  between operations  14.8 us (4%)
  loops' own time  11.9 us (3%)
    all_gather x1, waiting for transfers between devices, per_device(): lax.all_gather(key_rows, 'sp', axis=0, tiled=True)  54.6 us
    reduce_scatter x1, waiting for transfers between devices, per_device(): lax.psum_scatter((jnp.dot(attended, attend_proj, preferred_element_type=j...  51.2 us
    dot_general x13, matrix products, absorb(): jnp.einsum('hjqk,khe->hjqe', lifted.astype(jnp.bfloat16), values_here, pr...  35.5 us
    all_gather x1, waiting for transfers between devices, per_device(): lax.all_gather(tokens, 'tp', axis=1, tiled=True).astype(jnp.float32)  34.5 us
    all_gather x1, waiting for transfers between devices, per_device(): lax.all_gather(value_rows, 'sp', axis=0, tiled=True)  33.4 us
    dot_general x13, matrix products, absorb(): jnp.einsum('qgd,kgd->gqk', queries, key_block, preferred_element_type=jnp...  28.6 us
    dot_general x5, matrix products, per_device(): jnp.dot(scaled, weight, preferred_element_type=jnp.float32)  14.7 us
    reduce_sum x13, other arithmetic, absorb(): weight_sum = factor * weight_sum + jnp.sum(lifted, axis=3)  14.1 us
  transfers between devices with their start and end apart: 5, of which 4 were waited for; matrix products, arithmetic and copies ran while one was open for 37% of the time, Pallas kernels for 0%

commit v1 on v0

v1 whole, which is shorter than its diff:
```python
import functools

import jax
import jax.numpy as jnp
import numpy as np
from jax import lax
from jax.experimental import pallas as pl
from jax.experimental.pallas import tpu as pltpu
from jax.sharding import PartitionSpec as P

MESH = pl.DeviceIdType.MESH
BF = jnp.bfloat16
F32 = jnp.float32
ROPE_BASE = 500000.0
NORM_EPS = 1e-05
HEAD_KEEP = 0.8
MASKED = -1e30
LOG2E = float(np.log2(np.e))
LN2 = float(np.log(2.0))
NZ, NY, NX = 4, 4, 4
ROWS = 768
HD = 128
VD = 256
CH = 256
NCH = ROWS // CH
HALF = ROWS // 2
BLK = 96


def vmem():
    return pl.BlockSpec(memory_space=pltpu.VMEM)


def hbm():
    return pl.BlockSpec(memory_space=pl.ANY)


def remote(src, dst, ssem, rsem, dev):
    return pltpu.make_async_remote_copy(
        src_ref=src, dst_ref=dst, send_sem=ssem, recv_sem=rsem, device_id=dev, device_id_type=MESH
    )


def greet(devs):
    barrier = pltpu.get_barrier_semaphore()
    for dev in devs:
        pl.semaphore_signal(barrier, inc=1, device_id=dev, device_id_type=MESH)
    pl.semaphore_wait(barrier, len(devs))


def project_kernel(
    tok, gain, wq, wk, wv, wo, wi, ws, taps, rc, rs, oc, os_,
    q_out, kv_out, conv_out,
    xbuf, sc, wbuf, prod, outer, wsem, ssem, rsem, bsem,
):
    sp = lax.axis_index("sp")
    tp = lax.axis_index("tp")
    x = tp // 2
    c = tp % 2
    right = lax.rem(x + 1, NX) * 2 + c
    left = lax.rem(x + 3, NX) * 2 + c
    opp = lax.rem(x + 2, NX) * 2 + c
    mate = x * 2 + (1 - c)
    dr, dl, dm = (sp, right), (sp, left), (sp, mate)
    dn, dp = (lax.rem(sp + 1, NZ * NY), tp), (lax.rem(sp + NZ * NY - 1, NZ * NY), tp)
    weights = (wk, wv, wq, wi, ws, wo)
    wcopies = [pltpu.make_async_copy(w, wbuf.at[i], wsem.at[i]) for i, w in enumerate(weights)]
    for copy in wcopies:
        copy.start()
    greet([dr, dl, dm, dn, dp])

    def rows_of(k, part):
        if part is None:
            return pl.ds(k * CH, CH)
        return pl.ds(k * CH + part * (CH // 2), CH // 2)

    def own(k, kind, dev):
        return remote(
            tok.at[rows_of(k, None)], xbuf.at[tp, rows_of(k, None)],
            ssem.at[k, kind], rsem.at[k, kind], dev,
        )

    def pass_on(k, kind, block, part, dev):
        ref = xbuf.at[block, rows_of(k, part)]
        return remote(ref, ref, ssem.at[k, kind], rsem.at[k, kind], dev)

    sent = []

    def go(copy):
        copy.start()
        sent.append(copy)

    def send_own(k):
        go(own(k, 0, dr))
        go(own(k, 1, dl))
        go(own(k, 2, dm))

    def near(k):
        own(k, 0, dr).wait_recv()
        go(pass_on(k, 3, left, 0, dr))
        go(pass_on(k, 5, left, None, dm))
        own(k, 1, dl).wait_recv()
        go(pass_on(k, 4, right, 1, dl))
        go(pass_on(k, 6, right, None, dm))

    def far(k):
        pass_on(k, 3, left, 0, dr).wait_recv()
        go(pass_on(k, 7, opp, 0, dm))
        pass_on(k, 4, right, 1, dl).wait_recv()
        go(pass_on(k, 8, opp, 1, dm))

    def mates(k):
        own(k, 2, dm).wait_recv()
        pass_on(k, 5, left, None, dm).wait_recv()
        pass_on(k, 6, right, None, dm).wait_recv()
        pass_on(k, 7, opp, 0, dm).wait_recv()
        pass_on(k, 8, opp, 1, dm).wait_recv()

    send_own(0)
    send_own(1)
    xbuf[tp] = tok[...]
    co = oc[pl.ds(sp, 1), :]
    so = os_[pl.ds(sp, 1), :]

    def turn(v, k):
        c_r = rc[rows_of(k, None), :]
        s_r = rs[rows_of(k, None), :]
        cosine = co * c_r - so * s_r
        sine = so * c_r + co * s_r
        lane = lax.broadcasted_iota(jnp.int32, (CH, HD), 1)
        sine = jnp.where(lane < HD // 2, -sine, sine)
        parts = []
        for j in range(2):
            t = v[:, j * HD:(j + 1) * HD]
            parts.append(t * cosine + pltpu.roll(t, HD // 2, 1) * sine)
        return jnp.concatenate(parts, axis=1)

    def compute(k):
        rows = rows_of(k, None)
        square = jnp.zeros((CH, HD), F32)
        for b in range(2 * NX):
            xb = xbuf[b, rows, :].astype(F32)
            square += xb[:, :HD] * xb[:, :HD] + xb[:, HD:] * xb[:, HD:]
            sc[:, b * 256:(b + 1) * 256] = (xb * gain[:, b * 256:(b + 1) * 256]).astype(BF)
        total = jnp.sum(square, axis=1, keepdims=True)
        inv = lax.rsqrt(total / (2 * NX * 256) + NORM_EPS)

        def project(i):
            return inv * jnp.dot(sc[...], wbuf[i], preferred_element_type=F32)

        kv_out[rows, 0:VD] = turn(project(0), k).astype(BF)
        kv_out[rows, VD:2 * VD] = project(1).astype(BF)
        q_out[rows, :] = (turn(project(2), k) * (LOG2E * HD ** -0.5)).astype(BF)
        prod[pl.ds(8 + k * CH, CH), :] = project(3) * project(4)
        outer[rows, :] = project(5)

    near(0)
    near(1)
    send_own(2)
    far(0)
    mates(0)
    for copy in wcopies:
        copy.wait()
    compute(0)
    near(2)
    far(1)
    mates(1)
    compute(1)
    far(2)
    mates(2)
    compute(2)
    border = remote(
        prod.at[pl.ds(ROWS, 8)], prod.at[pl.ds(0, 8)], bsem.at[0], bsem.at[1], dn
    )
    border.start()
    border.wait_recv()
    border.wait_send()

    @pl.when(sp == 0)
    def _():
        prod[0:8, :] = jnp.zeros((8, 256), F32)

    tv = taps[...].astype(F32)
    smoothed = (
        tv[0:1] * prod[6:6 + ROWS, :] + tv[1:2] * prod[7:7 + ROWS, :] + tv[2:3] * prod[8:8 + ROWS, :]
    )
    conv_out[...] = (outer[...] * smoothed).astype(BF)
    for copy in sent:
        copy.wait_send()


def attend_kernel(
    lam, hgain, q_ref, kv_ref,
    att_ref, lse_ref,
    qb, kvb, m_ref, l_ref, acc, lt, stats, dbuf, relay, fin,
    qss, qrs, kss, krs, tss, trs, dss, drs,
):
    sp = lax.axis_index("sp")
    tp = lax.axis_index("tp")
    z = sp // NY
    y = sp % NY
    yr, yl, yo = lax.rem(y + 1, NY), lax.rem(y + 3, NY), lax.rem(y + 2, NY)
    zr, zl, zo = lax.rem(z + 1, NZ), lax.rem(z + 3, NZ), lax.rem(z + 2, NZ)
    dyr, dyl, dyo = (z * NY + yr, tp), (z * NY + yl, tp), (z * NY + yo, tp)
    dzr, dzl = (zr * NY + y, tp), (zl * NY + y, tp)
    greet([dyr, dyl, dyo, dzr, dzl])
    sent = []

    def go(copy):
        copy.start()
        sent.append(copy)

    def gather(src, buf, me, left, right, ss, rs, d_r, d_l):
        def part(h):
            return pl.ds(h * HALF, HALF)

        def own(h, kind, dev):
            return remote(src.at[part(h)], buf.at[me, part(h)], ss.at[kind], rs.at[kind], dev)

        def pass_on(block, h, kind, dev):
            ref = buf.at[block, part(h)]
            return remote(ref, ref, ss.at[kind], rs.at[kind], dev)

        copies = [
            own(0, 0, d_r), own(1, 1, d_r), own(1, 2, d_l), own(0, 3, d_l),
            pass_on(left, 0, 4, d_r), pass_on(right, 1, 5, d_l),
        ]
        for i in (0, 2, 1, 3):
            go(copies[i])

        def first():
            copies[0].wait_recv()
            go(copies[4])
            copies[2].wait_recv()
            go(copies[5])

        def second():
            copies[1].wait_recv()
            copies[3].wait_recv()

        def third():
            copies[4].wait_recv()
            copies[5].wait_recv()

        return first, second, third

    k1, k2, k3 = gather(kv_ref, kvb, z, zl, zr, kss, krs, dzr, dzl)
    q1, q2, q3 = gather(q_ref, qb, y, yl, yr, qss, qrs, dyr, dyl)
    qb[y] = q_ref[...]
    kvb[z] = kv_ref[...]
    m_ref[...] = jnp.full(m_ref.shape, MASKED, F32)
    l_ref[...] = jnp.zeros(l_ref.shape, F32)
    acc[...] = jnp.zeros(acc.shape, F32)

    def scores(qi, kj, r, tq, nk, j):
        q = qb[qi, pl.ds(r, tq), j * HD:(j + 1) * HD]
        k = kvb[kj, 0:nk, j * HD:(j + 1) * HD]
        return lax.dot_general(q, k, (((1,), (1,)), ((), ())), preferred_element_type=F32)

    def absorb(qi, kj, r, tq, nk, j, s):
        rows = pl.ds(r, tq)
        before = m_ref[j, qi, rows, :]
        now = jnp.maximum(before, jnp.max(s, axis=1, keepdims=True))
        fade = jnp.exp2(before - now)
        p = jnp.exp2(s - jnp.concatenate([now] * (nk // HD), axis=1))
        total = l_ref[j, qi, rows, :] * fade
        for i in range(nk // HD):
            total = total + p[:, i * HD:(i + 1) * HD]
        l_ref[j, qi, rows, :] = total
        m_ref[j, qi, rows, :] = now
        v = kvb[kj, 0:nk, VD:2 * VD]
        acc[j, qi, rows, :] = acc[j, qi, rows, :] * jnp.concatenate([fade] * 2, axis=1) + jnp.dot(
            p.astype(BF), v, preferred_element_type=F32
        )

    def full(qi, kj):
        s0 = scores(qi, kj, 0, ROWS, ROWS, 0)
        s1 = scores(qi, kj, 0, ROWS, ROWS, 1)
        absorb(qi, kj, 0, ROWS, ROWS, 0, s0)
        absorb(qi, kj, 0, ROWS, ROWS, 1, s1)

    def diagonal():
        for t in range(NCH):
            nk = (t + 1) * CH
            row = lax.broadcasted_iota(jnp.int32, (CH, nk), 0) + t * CH
            col = lax.broadcasted_iota(jnp.int32, (CH, nk), 1)
            ss = [scores(y, z, t * CH, CH, nk, j) for j in range(2)]
            for j in range(2):
                absorb(y, z, t * CH, CH, nk, j, jnp.where(col <= row, ss[j], MASKED))

    diagonal()
    q1()
    k1()
    q2()
    q3()

    def own_kv(i, _):
        qi = lax.rem(y + 1 + i, NY)

        @pl.when(qi > y)
        def _():
            full(qi, z)

        return 0

    lax.fori_loop(0, NY - 1, own_kv, 0)
    k2()

    def sweep(kj, least):
        @pl.when(z >= least)
        def _():
            def step(i, _):
                full(i, kj)
                return 0

            lax.fori_loop(0, NY, step, 0)

    sweep(zl, 1)
    sweep(zr, 3)
    k3()
    sweep(zo, 2)

    lane = lax.broadcasted_iota(jnp.int32, (ROWS, HD), 1)
    table = jnp.full((ROWS, HD), MASKED, F32)
    for qi in range(NY):
        for j in range(2):
            total = jnp.sum(l_ref[j, qi], axis=1, keepdims=True)
            lse = m_ref[j, qi] + jnp.log2(jnp.maximum(total, 1e-37))
            table = jnp.where(lane == 2 * qi + j, lse, table)
    stats[y] = jnp.transpose(table)[0:8, :]
    exchange = [
        remote(stats.at[y], stats.at[y], tss.at[i], trs.at[i], dev)
        for i, dev in enumerate((dyr, dyl, dyo))
    ]
    for copy in exchange:
        go(copy)
    for copy in exchange:
        copy.wait_recv()
    parts = [stats[i] for i in range(NY)]
    peak = jnp.maximum(jnp.maximum(parts[0], parts[1]), jnp.maximum(parts[2], parts[3]))
    whole = peak + jnp.log2(sum(jnp.exp2(p - peak) for p in parts))
    lt[...] = jnp.transpose(jnp.concatenate([whole, jnp.zeros((HD - 8, ROWS), F32)], axis=0))

    lam_v = lam[...]
    step_rows = 128

    def pick(rows, qi, j):
        lanes = lax.broadcasted_iota(jnp.int32, (step_rows, HD), 1)
        return jnp.sum(jnp.where(lanes == 2 * qi + j, lt[rows, :], 0.0), axis=1, keepdims=True)

    def share(rows, qi):
        outs = []
        for j in range(2):
            f = jnp.exp2(m_ref[j, qi, rows, :] - pick(rows, qi, j))
            outs.append(acc[j, qi, rows, :] * jnp.concatenate([f] * 2, axis=1))
        return outs[0] - lam_v * outs[1]

    def shares(qi):
        def one(i, _):
            rows = pl.ds(pl.multiple_of(i * step_rows, step_rows), step_rows)
            dbuf[qi, rows, :] = share(rows, qi).astype(BF)
            return 0

        lax.fori_loop(0, ROWS // step_rows, one, 0)

    h0, h1 = pl.ds(0, HALF), pl.ds(HALF, HALF)
    far = [
        remote(dbuf.at[yo, h0], relay.at[0], dss.at[0], drs.at[0], dyr),
        remote(dbuf.at[yo, h1], relay.at[1], dss.at[1], drs.at[1], dyl),
    ]
    near = [
        remote(dbuf.at[yr, h1], fin.at[0, h1], dss.at[2], drs.at[2], dyr),
        remote(dbuf.at[yl, h0], fin.at[1, h0], dss.at[3], drs.at[3], dyl),
        remote(dbuf.at[yr, h0], fin.at[0, h0], dss.at[4], drs.at[4], dyr),
        remote(dbuf.at[yl, h1], fin.at[1, h1], dss.at[5], drs.at[5], dyl),
    ]
    shares(yo)
    go(far[0])
    go(far[1])
    shares(yr)
    shares(yl)
    go(near[0])
    go(near[1])
    far[0].wait_recv()
    dbuf[yr, h0, :] = (dbuf[yr, h0, :].astype(F32) + relay[0].astype(F32)).astype(BF)
    go(near[2])
    far[1].wait_recv()
    dbuf[yl, h1, :] = (dbuf[yl, h1, :].astype(F32) + relay[1].astype(F32)).astype(BF)
    go(near[3])
    for copy in near:
        copy.wait_recv()

    def last(i, _):
        rows = pl.ds(pl.multiple_of(i * step_rows, step_rows), step_rows)
        d = share(rows, y) + fin[0, rows, :].astype(F32) + fin[1, rows, :].astype(F32)
        back = lax.rsqrt(jnp.mean(d * d, axis=1, keepdims=True) + NORM_EPS)
        att_ref[rows, :] = (d * back * hgain[...] * HEAD_KEEP).astype(BF)
        lse_ref[rows, 0:1] = pick(rows, y, 0) * LN2
        lse_ref[rows, 1:2] = pick(rows, y, 1) * LN2
        return 0

    lax.fori_loop(0, ROWS // step_rows, last, 0)
    for copy in sent:
        copy.wait_send()


def merge_kernel(
    att, conv, ap, cp,
    out,
    part, precv, relay, fin, apb, cpb,
    wsem, pss, prs, rss, rrs,
):
    sp = lax.axis_index("sp")
    tp = lax.axis_index("tp")
    x = tp // 2
    c = tp % 2
    xr, xl, xo = lax.rem(x + 1, NX), lax.rem(x + 3, NX), lax.rem(x + 2, NX)
    dr, dl, dm = (sp, xr * 2 + c), (sp, xl * 2 + c), (sp, x * 2 + (1 - c))
    loads = [pltpu.make_async_copy(ap, apb, wsem.at[0]), pltpu.make_async_copy(cp, cpb, wsem.at[1])]
    for copy in loads:
        copy.start()
    greet([dr, dl, dm])
    for copy in loads:
        copy.wait()
    sent = []

    def go(copy):
        copy.start()
        sent.append(copy)

    cols = 512
    order = (xo, xr, xl, x)
    mates = [
        remote(part.at[xx * 2 + (1 - c)], precv.at[xx], pss.at[i], prs.at[i], dm)
        for i, xx in enumerate(order)
    ]

    def compute(xx):
        rows = pl.ds(pl.multiple_of(xx * (2 * BLK), 2 * BLK), 2 * BLK)
        a = att[rows, :]
        b = conv[rows, :]
        for n in range(2048 // cols):
            cs = slice(n * cols, (n + 1) * cols)
            p = jnp.dot(a, apb[:, cs], preferred_element_type=F32) + jnp.dot(
                b, cpb[:, cs], preferred_element_type=F32
            )
            p = p.astype(BF)
            part[xx * 2, :, cs] = p[:BLK]
            part[xx * 2 + 1, :, cs] = p[BLK:]

    def join(xx, rows, extra):
        t = part[xx * 2 + c, rows, :].astype(F32) + precv[xx, rows, :].astype(F32)
        if extra is not None:
            t = t + extra[...].astype(F32)
        part[xx * 2 + c, rows, :] = t.astype(BF)

    h0, h1 = pl.ds(0, BLK // 2), pl.ds(BLK // 2, BLK // 2)
    io, ir, il = xo * 2 + c, xr * 2 + c, xl * 2 + c
    far = [
        remote(part.at[io, h0], relay.at[0], rss.at[0], rrs.at[0], dr),
        remote(part.at[io, h1], relay.at[1], rss.at[1], rrs.at[1], dl),
    ]
    near = [
        remote(part.at[ir, h1], fin.at[0, h1], rss.at[2], rrs.at[2], dr),
        remote(part.at[il, h0], fin.at[1, h0], rss.at[3], rrs.at[3], dl),
        remote(part.at[ir, h0], fin.at[0, h0], rss.at[4], rrs.at[4], dr),
        remote(part.at[il, h1], fin.at[1, h1], rss.at[5], rrs.at[5], dl),
    ]
    compute(xo)
    go(mates[0])
    compute(xr)
    go(mates[1])
    mates[0].wait_recv()
    join(xo, h0, None)
    join(xo, h1, None)
    go(far[0])
    go(far[1])
    compute(xl)
    go(mates[2])
    mates[1].wait_recv()
    join(xr, h1, None)
    go(near[0])
    compute(x)
    go(mates[3])
    mates[2].wait_recv()
    join(xl, h0, None)
    go(near[1])
    far[0].wait_recv()
    join(xr, h0, relay.at[0])
    go(near[2])
    far[1].wait_recv()
    join(xl, h1, relay.at[1])
    go(near[3])
    mates[3].wait_recv()
    for copy in near:
        copy.wait_recv()
    out[...] = (
        part[tp].astype(F32) + precv[x].astype(F32) + fin[0].astype(F32) + fin[1].astype(F32)
    ).astype(BF)
    for copy in sent:
        copy.wait_send()


def tables():
    inverse = ROPE_BASE ** (-np.arange(HD // 2, dtype=np.float64) * 2.0 / HD)
    inverse = inverse.astype(np.float32).astype(np.float64)
    inverse = np.concatenate([inverse, inverse])
    local = np.arange(ROWS)[:, None] * inverse[None, :]
    offset = (np.arange(NZ * NY) * ROWS)[:, None] * inverse[None, :]
    return [f(a).astype(np.float32) for a in (local, offset) for f in (np.cos, np.sin)]


def params(cid):
    return pltpu.CompilerParams(
        collective_id=cid, has_side_effects=True, vmem_limit_bytes=60 * 2 ** 20
    )


DMA = pltpu.SemaphoreType.DMA


def per_device(
    tokens, norm_gain, w_query, w_key, w_value, w_outer, w_inner, w_signal,
    conv_taps, lambdas, head_gain, attend_proj, convolve_proj,
):
    rc, rs, oc, os_ = tables()
    q, kv, conv = pl.pallas_call(
        project_kernel,
        out_shape=(
            jax.ShapeDtypeStruct((ROWS, VD), BF),
            jax.ShapeDtypeStruct((ROWS, 2 * VD), BF),
            jax.ShapeDtypeStruct((ROWS, 256), BF),
        ),
        in_specs=[vmem(), vmem()] + [hbm()] * 6 + [vmem()] * 5,
        out_specs=(vmem(), vmem(), vmem()),
        scratch_shapes=[
            pltpu.VMEM((2 * NX, ROWS, 256), BF),
            pltpu.VMEM((CH, 2048), BF),
            pltpu.VMEM((6, 2048, 256), BF),
            pltpu.VMEM((ROWS + 8, 256), F32),
            pltpu.VMEM((ROWS, 256), F32),
            DMA((6,)), DMA((NCH, 9)), DMA((NCH, 9)), DMA((2,)),
        ],
        compiler_params=params(1),
        name="project",
    )(
        tokens, norm_gain.reshape(1, -1), w_query, w_key, w_value, w_outer, w_inner, w_signal,
        conv_taps, rc, rs, oc, os_,
    )
    att, lse = pl.pallas_call(
        attend_kernel,
        out_shape=(
            jax.ShapeDtypeStruct((ROWS, VD), BF),
            jax.ShapeDtypeStruct((ROWS, 2), F32),
        ),
        in_specs=[vmem()] * 4,
        out_specs=(vmem(), vmem()),
        scratch_shapes=[
            pltpu.VMEM((NY, ROWS, VD), BF),
            pltpu.VMEM((NZ, ROWS, 2 * VD), BF),
            pltpu.VMEM((2, NY, ROWS, HD), F32),
            pltpu.VMEM((2, NY, ROWS, HD), F32),
            pltpu.VMEM((2, NY, ROWS, VD), F32),
            pltpu.VMEM((ROWS, HD), F32),
            pltpu.VMEM((NY, 8, ROWS), F32),
            pltpu.VMEM((NY, ROWS, VD), BF),
            pltpu.VMEM((2, HALF, VD), BF),
            pltpu.VMEM((2, ROWS, VD), BF),
            DMA((6,)), DMA((6,)), DMA((6,)), DMA((6,)), DMA((3,)), DMA((3,)), DMA((6,)), DMA((6,)),
        ],
        compiler_params=params(2),
        name="attend",
    )(lambdas.reshape(1, 1), head_gain.reshape(1, -1), q, kv)
    mixed = pl.pallas_call(
        merge_kernel,
        out_shape=jax.ShapeDtypeStruct((BLK, 2048), BF),
        in_specs=[vmem(), vmem(), hbm(), hbm()],
        out_specs=vmem(),
        scratch_shapes=[
            pltpu.VMEM((2 * NX, BLK, 2048), BF),
            pltpu.VMEM((NX, BLK, 2048), BF),
            pltpu.VMEM((2, BLK // 2, 2048), BF),
            pltpu.VMEM((2, BLK, 2048), BF),
            pltpu.VMEM((256, 2048), BF),
            pltpu.VMEM((256, 2048), BF),
            DMA((2,)), DMA((4,)), DMA((4,)), DMA((6,)), DMA((6,)),
        ],
        compiler_params=params(3),
        name="merge",
    )(att, conv, attend_proj, convolve_proj)
    return mixed, lse


def solution(mesh):
    return jax.shard_map(
        per_device,
        mesh=mesh,
        in_specs=(
            P("sp", "tp"), P(), P(None, "tp"), P(None, "tp"), P(None, "tp"), P(None, "tp"),
            P(None, "tp"), P(None, "tp"), P(None, "tp"), P("tp"), P(), P("tp", None), P("tp", None),
        ),
        out_specs=(P(("sp", "tp"), None), P("sp", "tp")),
        check_vma=False,
    )
```

time: 356 us -> 121 us (0.34); the launches traced: 351 us -> 121 us
  waiting for transfers between devices: 174 us -> 0 us
  Pallas kernels: 0 us -> 118 us
  matrix products: 90.9 us -> 0 us
  other arithmetic: 30.5 us -> 0 us
  local copies, waits for them, and re-layouts: 24.8 us -> 1.74 us
  between operations: 14.8 us -> 1.33 us
  loops' own time: 11.9 us -> 0 us
    all_gather x3 -> x0, waiting for transfers between devices: 122 us -> none  [the longest x1 54.6 us: per_device(): lax.all_gather(key_rows, 'sp', axis=0, tiled=True)]
    pallas_call x0 -> x3, Pallas kernels: none -> 118 us  [the longest x1 63.6 us: per_device(): pl.pallas_call(attend_kernel, out_shape=(jax.ShapeDtypeStruct((ROWS, VD),...]
    dot_general x33 -> x0, matrix products: 90.9 us -> none  [the longest x13 35.5 us: absorb(): jnp.einsum('hjqk,khe->hjqe', lifted.astype(jnp.bfloat16), values_here, pr...]
    reduce_scatter x1 -> x0, waiting for transfers between devices: 51.2 us -> none  [per_device(): lax.psum_scatter((jnp.dot(attended, attend_proj, preferred_element_type=j...]
    reduce_sum x15 -> x0, other arithmetic: 16.9 us -> none  [the longest x13 14.1 us: absorb(): weight_sum = factor * weight_sum + jnp.sum(lifted, axis=3)]
    unnamed x29 -> x6, local copies, waits for them, and re-layouts: 13.7 us -> 1.74 us
    another operation x17 -> x0, loops' own time: 11.9 us -> none  [the longest x1 10.9 us: make_fold(): lax.scan(one_shard, carry, jnp.arange(shard_count, dtype=jnp.int32))]
    dynamic_slice x16 -> x0, local copies, waits for them, and re-layouts: 9.79 us -> none  [make_fold(): lax.scan(one_shard, carry, jnp.arange(shard_count, dtype=jnp.int32))]
  transfers between devices with their start and end apart: 5 -> 0, of which waited for: 4 -> 0; matrix products, arithmetic and copies ran while one was open for 37% -> 0% of each run, Pallas kernels for 0% -> 0%
where the time goes in v1:
time: 121 us
  Pallas kernels  118 us (98%)
  local copies, waits for them, and re-layouts  1.74 us (1%)
  between operations  1.33 us (1%)
    pallas_call x1, Pallas kernels, per_device(): pl.pallas_call(attend_kernel, out_shape=(jax.ShapeDtypeStruct((ROWS, VD),...  63.6 us
    pallas_call x1, Pallas kernels, per_device(): pl.pallas_call(project_kernel, out_shape=(jax.ShapeDtypeStruct((ROWS, VD)...  29.3 us
    pallas_call x1, Pallas kernels, per_device(): pl.pallas_call(merge_kernel, out_shape=jax.ShapeDtypeStruct((BLK, 2048),...  25 us

profile of v1, /device:TPU:97, one launch (start us, length us, event | category | flops | bytes accessed | tf_op | source)
XLA Modules:
  0.0 121.0 jit_solution(12182625816272896565)
XLA Ops:
  1.3 29.3 %project.1 = (bf16[768,256]{1,0:T(8,128)(2,1)}, bf16[768,512]{1,0:T(8,128)(2,1)}, bf16[768,256]{1,0:T(8,128)(2,1)}) custom-call(bf16[768,256]{1,0:T(8,128)(2,1)} %tok.1, f32[1,2048]{1,0:T(1,128)} %bitcast.4, bf16[2048,256]{1,0:T(8,128)(2,1)} %wq.1, bf16[2048,256]{1,0:T(8,128)(2,1)} %wk.1, bf16[2048,256]{1,0:T(8,128)(2,1)} %wv.1, bf16[2048,256]{1,0:T(8,128)(2,1)} %wo.1, ...), custom_call_target="tpu_custom_call" | custom-call | tf_op jit(solution)/shard_map/project/pallas_call | solution.py:527
  30.6 63.6 %attend.1 = (bf16[768,256]{1,0:T(8,128)(2,1)}, f32[768,2]{1,0:T(8,128)}) custom-call(f32[1,1]{1,0:T(1,128)} %bitcast.3.lam, f32[1,256]{1,0:T(1,128)} %bitcast.5, bf16[768,256]{1,0:T(8,128)(2,1)} %get-tuple-element.7.q_ref, bf16[768,512]{1,0:T(8,128)(2,1)} %get-tuple-element.8.kv_ref), custom_call_target="tpu_custom_call" | custom-call | tf_op jit(solution)/shard_map/attend/pallas_call | solution.py:550
  94.2 0.0 copy-start.1
  94.2 25.0 %merge.1 = bf16[96,2048]{1,0:T(8,128)(2,1)} custom-call(bf16[768,256]{1,0:T(8,128)(2,1)} %get-tuple-element.9.att, bf16[768,256]{1,0:T(8,128)(2,1)} %get-tuple-element.10.conv, bf16[256,2048]{1,0:T(8,128)(2,1)} %ap.1, bf16[256,2048]{1,0:T(8,128)(2,1)} %cp.1), custom_call_target="tpu_custom_call" | custom-call | tf_op jit(solution)/shard_map/merge/pallas_call | solution.py:574
  119.3 0.0 copy-done.1
  119.3 0.0 copy-start
  119.3 0.7 copy.19
  120.0 0.2 copy-done
  120.3 0.7 copy.22
Async XLA Ops:
  94.2 25.1 %copy-start.1 = (f32[768,2]{1,0:T(8,128)S(1)}, f32[768,2]{1,0:T(8,128)}, u32[]{:S(2)}) copy-start(f32[768,2]{1,0:T(8,128)} %get-tuple-element.13) | copy-start | bytes 18436
  119.3 1.0 copy-start

commit v2 on v0

v2 whole, which is shorter than its diff:
```python
import functools

import jax
import jax.numpy as jnp
import numpy as np
from jax import lax
from jax.experimental import pallas as pl
from jax.experimental.pallas import tpu as pltpu
from jax.sharding import PartitionSpec as P

MESH = pl.DeviceIdType.MESH
BF = jnp.bfloat16
F32 = jnp.float32
ROPE_BASE = 500000.0
NORM_EPS = 1e-05
HEAD_KEEP = 0.8
MASKED = -1e30
LOG2E = float(np.log2(np.e))
LN2 = float(np.log(2.0))
NZ, NY, NX = 4, 4, 4
ROWS = 768
HD = 128
VD = 256
CH = 256
NCH = ROWS // CH
HF = CH // 2
PC = 32
BLK = 96


def vmem():
    return pl.BlockSpec(memory_space=pltpu.VMEM)


def hbm():
    return pl.BlockSpec(memory_space=pl.ANY)


def remote(src, dst, ssem, rsem, dev):
    return pltpu.make_async_remote_copy(
        src_ref=src, dst_ref=dst, send_sem=ssem, recv_sem=rsem, device_id=dev, device_id_type=MESH
    )


def scope(name):
    return jax.named_scope(name)


def greet(devs):
    barrier = pltpu.get_barrier_semaphore()
    for dev in devs:
        pl.semaphore_signal(barrier, inc=1, device_id=dev, device_id_type=MESH)
    pl.semaphore_wait(barrier, len(devs))


def layer_kernel(
    tok, gain, lam, hgain, taps, rc, rs, oc, os_, wq, wk, wv, wo, wi, ws, ap, cp,
    out, lse_ref,
    xbuf, sc, wbuf, apb, cpb, prod, outer, conv,
    qb, kvb, m_ref, l_ref, acc, lt, stats, dbuf, relay, fin,
    part, precv, xrelay, xfin,
    wsem, bsem, gss, grs, kss, krs, qss, qrs, tss, trs, dss, drs, pss, prs, xss, xrs,
):
    sp = lax.axis_index("sp")
    tp = lax.axis_index("tp")
    x, c = tp // 2, tp % 2
    z, y = sp // NY, sp % NY
    xr, xl, xo = lax.rem(x + 1, NX), lax.rem(x + 3, NX), lax.rem(x + 2, NX)
    yr, yl, yo = lax.rem(y + 1, NY), lax.rem(y + 3, NY), lax.rem(y + 2, NY)
    zr, zl, zo = lax.rem(z + 1, NZ), lax.rem(z + 3, NZ), lax.rem(z + 2, NZ)
    dxr, dxl, dm = (sp, xr * 2 + c), (sp, xl * 2 + c), (sp, x * 2 + (1 - c))
    dyr, dyl, dyo = (z * NY + yr, tp), (z * NY + yl, tp), (z * NY + yo, tp)
    dzr, dzl = (zr * NY + y, tp), (zl * NY + y, tp)
    dn, dp = (lax.rem(sp + 1, NZ * NY), tp), (lax.rem(sp + NZ * NY - 1, NZ * NY), tp)
    right, left, opp = xr * 2 + c, xl * 2 + c, xo * 2 + c

    weights = ((wk, wbuf.at[0]), (wv, wbuf.at[1]), (wq, wbuf.at[2]), (wi, wbuf.at[3]),
               (ws, wbuf.at[4]), (wo, wbuf.at[5]), (ap, apb), (cp, cpb))
    wcopies = [pltpu.make_async_copy(a, b, wsem.at[i]) for i, (a, b) in enumerate(weights)]
    for copy in wcopies:
        copy.start()
    for k in range(NCH):
        for t in range(2 * NX):
            xbuf[tp, k * CH + t * PC:k * CH + (t + 1) * PC, :] = tok[t * BLK + k * PC:t * BLK + (k + 1) * PC, :]
    with scope("greet"):
        greet([dxr, dxl, dm, dyr, dyl, dyo, dzr, dzl, dn, dp])
    sent = []

    def go(copy):
        copy.start()
        sent.append(copy)

    def rows_of(k, h=None):
        return pl.ds(k * CH, CH) if h is None else pl.ds(k * CH + h * HF, HF)

    def pass_on(k, kind, block, h, dev):
        ref = xbuf.at[block, rows_of(k, h)]
        return remote(ref, ref, gss.at[k, kind], grs.at[k, kind], dev)

    def send_own(k):
        go(pass_on(k, 0, tp, None, dxr))
        go(pass_on(k, 1, tp, None, dxl))
        go(pass_on(k, 2, tp, None, dm))

    def near(k):
        pass_on(k, 0, tp, None, dxr).wait_recv()
        go(pass_on(k, 3, left, 0, dxr))
        go(pass_on(k, 5, left, None, dm))
        pass_on(k, 1, tp, None, dxl).wait_recv()
        go(pass_on(k, 4, right, 1, dxl))
        go(pass_on(k, 6, right, None, dm))

    def far(k):
        pass_on(k, 3, left, 0, dxr).wait_recv()
        go(pass_on(k, 7, opp, 0, dm))
        pass_on(k, 4, right, 1, dxl).wait_recv()
        go(pass_on(k, 8, opp, 1, dm))

    def mates(k):
        pass_on(k, 2, tp, None, dm).wait_recv()
        pass_on(k, 5, left, None, dm).wait_recv()
        pass_on(k, 6, right, None, dm).wait_recv()
        pass_on(k, 7, opp, 0, dm).wait_recv()
        pass_on(k, 8, opp, 1, dm).wait_recv()

    def ring(buf, me, lf, rt, ss, rs_, d_r, d_l):
        def one(block, k, h, kind, dev):
            ref = buf.at[block, rows_of(k, h)]
            return remote(ref, ref, ss.at[k, kind], rs_.at[k, kind], dev)

        return [
            [one(me, k, 0, 0, d_r), one(me, k, 1, 1, d_r), one(me, k, 1, 2, d_l),
             one(me, k, 0, 3, d_l), one(lf, k, 0, 4, d_r), one(rt, k, 1, 5, d_l)]
            for k in range(NCH)
        ]

    kring = ring(kvb, z, zl, zr, kss, krs, dzr, dzl)
    qring = ring(qb, y, yl, yr, qss, qrs, dyr, dyl)

    def ring_send(copies):
        for i in (0, 2, 1, 3):
            go(copies[i])

    def ring_relay(copies):
        copies[0].wait_recv()
        go(copies[4])
        copies[2].wait_recv()
        go(copies[5])

    def ring_rest(rings):
        for copies in rings:
            copies[1].wait_recv()
            copies[3].wait_recv()

    def ring_far(rings):
        for copies in rings:
            copies[4].wait_recv()
            copies[5].wait_recv()

    co = oc[pl.ds(sp, 1), :]
    so = os_[pl.ds(sp, 1), :]

    def compute(k):
        rows = rows_of(k)
        square = jnp.zeros((CH, HD), F32)
        for b in range(2 * NX):
            xb = xbuf[b, rows, :].astype(F32)
            square += xb[:, :HD] * xb[:, :HD] + xb[:, HD:] * xb[:, HD:]
            sc[:, b * 256:(b + 1) * 256] = (xb * gain[:, b * 256:(b + 1) * 256]).astype(BF)
        total = jnp.sum(square, axis=1, keepdims=True)
        inv = lax.rsqrt(total / (2 * NX * 256) + NORM_EPS)
        c_r, s_r = rc[rows, :], rs[rows, :]
        cosine = co * c_r - so * s_r
        sine = so * c_r + co * s_r
        lane = lax.broadcasted_iota(jnp.int32, (CH, HD), 1)
        sine = jnp.where(lane < HD // 2, -sine, sine)

        def project(i):
            return inv * jnp.dot(sc[...], wbuf[i], preferred_element_type=F32)

        def turn(v):
            parts = []
            for j in range(2):
                t = v[:, j * HD:(j + 1) * HD]
                parts.append(t * cosine + pltpu.roll(t, HD // 2, 1) * sine)
            return jnp.concatenate(parts, axis=1)

        kvb[z, rows, 0:VD] = turn(project(0)).astype(BF)
        kvb[z, rows, VD:2 * VD] = project(1).astype(BF)
        qb[y, rows, :] = (turn(project(2)) * (LOG2E * HD ** -0.5)).astype(BF)
        ring_send(kring[k])
        ring_send(qring[k])
        pr = project(3) * project(4)
        og = project(5)
        for t in range(2 * NX):
            at = t * BLK + k * PC
            prod[8 + at:8 + at + PC, :] = pr[t * PC:(t + 1) * PC]
            outer[at:at + PC, :] = og[t * PC:(t + 1) * PC]

    def scores(qi, kj, rows, j):
        q = qb[qi, rows, j * HD:(j + 1) * HD]
        k = kvb[kj, :, j * HD:(j + 1) * HD]
        return lax.dot_general(q, k, (((1,), (1,)), ((), ())), preferred_element_type=F32)

    def absorb(qi, kj, rows, j, s):
        before = m_ref[j, qi, rows, :]
        now = jnp.maximum(before, jnp.max(s, axis=1, keepdims=True))
        fade = jnp.exp2(before - now)
        p = jnp.exp2(s - jnp.concatenate([now] * (ROWS // HD), axis=1))
        total = l_ref[j, qi, rows, :] * fade
        for i in range(ROWS // HD):
            total = total + p[:, i * HD:(i + 1) * HD]
        l_ref[j, qi, rows, :] = total
        m_ref[j, qi, rows, :] = now
        acc[j, qi, rows, :] = acc[j, qi, rows, :] * jnp.concatenate([fade] * 2, axis=1) + jnp.dot(
            p.astype(BF), kvb[kj, :, VD:2 * VD], preferred_element_type=F32
        )

    def attend(qi, kj, rows, mask=None):
        ss = [scores(qi, kj, rows, j) for j in range(2)]
        for j in range(2):
            s = ss[j] if mask is None else jnp.where(mask, ss[j], MASKED)
            absorb(qi, kj, rows, j, s)

    def place(p):
        return ((p >> 5) & 7) * BLK + (p >> 8) * PC + (p & 31)

    def own_pair():
        row = place(lax.broadcasted_iota(jnp.int32, (ROWS, HD), 0))
        row = jnp.concatenate([row] * (ROWS // HD), axis=1)
        col = place(lax.broadcasted_iota(jnp.int32, (1, ROWS), 1))
        attend(y, z, pl.ds(0, ROWS), col <= row)

    def start():
        m_ref[...] = jnp.full(m_ref.shape, MASKED, F32)
        l_ref[...] = jnp.zeros(l_ref.shape, F32)
        acc[...] = jnp.zeros(acc.shape, F32)

    send_own(0)
    send_own(1)
    start()
    with scope("near0"):
        near(0)
    with scope("near1"):
        near(1)
    send_own(2)
    with scope("far0"):
        far(0)
    with scope("mates0"):
        mates(0)
        for copy in wcopies:
            copy.wait()
    with scope("comp0"):
        compute(0)
    with scope("near2"):
        near(2)
    with scope("far1"):
        far(1)
        mates(1)
    with scope("comp1"):
        compute(1)
    with scope("far2"):
        far(2)
        mates(2)
    with scope("qrel0"):
        ring_relay(qring[0])
    with scope("comp2"):
        compute(2)
    border = remote(prod.at[pl.ds(ROWS, 8)], prod.at[pl.ds(0, 8)], bsem.at[0], bsem.at[1], dn)
    go(border)
    with scope("rel0"):
        ring_relay(kring[0])
        ring_relay(qring[1])
    with scope("own"):
        own_pair()
    with scope("rel1"):
        ring_relay(kring[1])
        ring_relay(qring[2])
    with scope("conv"):
        border.wait_recv()

        @pl.when(sp == 0)
        def _():
            prod[0:8, :] = jnp.zeros((8, 256), F32)

        tv = taps[...].astype(F32)
        smoothed = (
            tv[0:1] * prod[6:6 + ROWS, :] + tv[1:2] * prod[7:7 + ROWS, :] + tv[2:3] * prod[8:8 + ROWS, :]
        )
        conv[...] = (outer[...] * smoothed).astype(BF)
    with scope("qrest"):
        ring_rest(qring)

    def step(i, _):
        @pl.when(i == 2)
        def _():
            with scope("qfar"):
                ring_far(qring)
            with scope("rel2"):
                ring_relay2()

        @pl.when(i == 3)
        def _():
            with scope("krest"):
                ring_rest(kring)

        mine = i < 3
        first = i < 7
        turn_ = jnp.where(i == 0, 1, jnp.where(i == 1, 3, 2))
        qi = jnp.where(mine, lax.rem(y + turn_, NY), lax.rem(i + 1, NY))
        kj = jnp.where(mine, z, jnp.where(first, zl, zr))
        need = (mine & (qi > y)) | (~mine & first & (z >= 1)) | (~first & (z == 3))

        @pl.when(need)
        def _():
            with scope("item"):
                attend(qi, kj, pl.ds(0, ROWS))

        return 0

    def ring_relay2():
        copies = kring[2]
        copies[0].wait_recv()
        copies[4].start()
        copies[2].wait_recv()
        copies[5].start()

    lax.fori_loop(0, 11, step, 0)
    sent.append(kring[2][4])
    sent.append(kring[2][5])
    with scope("kfar"):
        ring_far(kring)

    lam_v = lam[...]

    def last_keys(k):
        @pl.when(z >= 2)
        def _():
            ss = [[scores(qi, zo, rows_of(k), j) for qi in range(NY)] for j in range(2)]
            for j in range(2):
                for qi in range(NY):
                    absorb(qi, zo, rows_of(k), j, ss[j][qi])

    def stat_copies(k):
        ref = stats.at[y, k]
        return [
            remote(ref, ref, tss.at[k, i], trs.at[k, i], dev) for i, dev in enumerate((dyr, dyl, dyo))
        ]

    def send_stats(k):
        rows = rows_of(k)
        lane = lax.broadcasted_iota(jnp.int32, (CH, HD), 1)
        table = jnp.full((CH, HD), MASKED, F32)
        for qi in range(NY):
            for j in range(2):
                total = jnp.sum(l_ref[j, qi, rows, :], axis=1, keepdims=True)
                lse = m_ref[j, qi, rows, :] + jnp.log2(jnp.maximum(total, 1e-37))
                table = jnp.where(lane == 2 * qi + j, lse, table)
        stats[y, k] = jnp.transpose(table)[0:8, :]
        for copy in stat_copies(k):
            go(copy)

    def pick(rows, qi, j):
        lanes = lax.broadcasted_iota(jnp.int32, (CH, HD), 1)
        return jnp.sum(jnp.where(lanes == 2 * qi + j, lt[rows, :], 0.0), axis=1, keepdims=True)

    def share(rows, qi):
        outs = []
        for j in range(2):
            f = jnp.exp2(m_ref[j, qi, rows, :] - pick(rows, qi, j))
            outs.append(acc[j, qi, rows, :] * jnp.concatenate([f] * 2, axis=1))
        return outs[0] - lam_v * outs[1]

    def scatter(k):
        h0, h1 = rows_of(k, 0), rows_of(k, 1)
        at = pl.ds(k * HF, HF)
        pairs = [
            (dbuf.at[yo, h0], relay.at[0, at], dyr),
            (dbuf.at[yo, h1], relay.at[1, at], dyl),
            (dbuf.at[yr, h1], fin.at[0, h1], dyr),
            (dbuf.at[yl, h0], fin.at[1, h0], dyl),
            (dbuf.at[yr, h0], fin.at[0, h0], dyr),
            (dbuf.at[yl, h1], fin.at[1, h1], dyl),
        ]
        return [remote(a, b, dss.at[k, i], drs.at[k, i], d) for i, (a, b, d) in enumerate(pairs)]

    def send_shares(k):
        rows = rows_of(k)
        for copy in stat_copies(k):
            copy.wait_recv()
        parts = [stats[i, k] for i in range(NY)]
        peak = jnp.maximum(jnp.maximum(parts[0], parts[1]), jnp.maximum(parts[2], parts[3]))
        whole = peak + jnp.log2(sum(jnp.exp2(p - peak) for p in parts))
        lt[rows, :] = jnp.transpose(jnp.concatenate([whole, jnp.zeros((HD - 8, CH), F32)], axis=0))

        def one(i, _):
            qi = lax.rem(y + jnp.where(i == 0, 2, jnp.where(i == 1, 1, 3)), NY)
            dbuf[qi, rows, :] = share(rows, qi).astype(BF)
            return 0

        lax.fori_loop(0, NY - 1, one, 0)
        for copy in scatter(k)[:4]:
            go(copy)

    def join_shares(k):
        copies = scatter(k)
        h0, h1 = rows_of(k, 0), rows_of(k, 1)
        at = pl.ds(k * HF, HF)
        copies[0].wait_recv()
        dbuf[yr, h0, :] = (dbuf[yr, h0, :].astype(F32) + relay[0, at, :].astype(F32)).astype(BF)
        go(copies[4])
        copies[1].wait_recv()
        dbuf[yl, h1, :] = (dbuf[yl, h1, :].astype(F32) + relay[1, at, :].astype(F32)).astype(BF)
        go(copies[5])

    def mate_copy(k):
        return remote(part.at[k, 1 - c], precv.at[k], pss.at[k], prs.at[k], dm)

    def merge(k):
        rows = rows_of(k)
        for copy in scatter(k)[2:]:
            copy.wait_recv()
        d = share(rows, y) + fin[0, rows, :].astype(F32) + fin[1, rows, :].astype(F32)
        back = lax.rsqrt(jnp.mean(d * d, axis=1, keepdims=True) + NORM_EPS)
        att = (d * back * hgain[...] * HEAD_KEEP).astype(BF)
        ls = [pick(rows, y, j) * LN2 for j in range(2)]
        pieces = [slice(t * BLK + k * PC, t * BLK + (k + 1) * PC) for t in range(2 * NX)]
        for t in range(2 * NX):
            for j in range(2):
                lse_ref[pieces[t], j:j + 1] = ls[j][t * PC:(t + 1) * PC]
        con = jnp.concatenate([conv[pieces[t], :] for t in range(2 * NX)], axis=0)
        cols = 512
        for n in range(2048 // cols):
            cs = slice(n * cols, (n + 1) * cols)
            p = jnp.dot(att, apb[:, cs], preferred_element_type=F32) + jnp.dot(
                con, cpb[:, cs], preferred_element_type=F32
            )
            p = p.astype(BF)
            for t in range(2 * NX):
                part[k, t % 2, t // 2, :, cs] = p[t * PC:(t + 1) * PC]
        go(mate_copy(k))

    g0, g1 = pl.ds(0, PC // 2), pl.ds(PC // 2, PC // 2)

    def spread(k):
        pairs = [
            (part.at[k, c, xo, g0], xrelay.at[k, 0], dxr),
            (part.at[k, c, xo, g1], xrelay.at[k, 1], dxl),
            (part.at[k, c, xr, g1], xfin.at[k, 0, g1], dxr),
            (part.at[k, c, xl, g0], xfin.at[k, 1, g0], dxl),
            (part.at[k, c, xr, g0], xfin.at[k, 0, g0], dxr),
            (part.at[k, c, xl, g1], xfin.at[k, 1, g1], dxl),
        ]
        return [remote(a, b, xss.at[k, i], xrs.at[k, i], d) for i, (a, b, d) in enumerate(pairs)]

    def add_mate(k, xx, g, extra=None):
        t = part[k, c, xx, g, :].astype(F32) + precv[k, xx, g, :].astype(F32)
        if extra is not None:
            t = t + extra.astype(F32)
        part[k, c, xx, g, :] = t.astype(BF)

    def send_sums(k):
        copies = spread(k)
        mate_copy(k).wait_recv()
        add_mate(k, xo, pl.ds(0, PC))
        add_mate(k, xr, g1)
        add_mate(k, xl, g0)
        for copy in copies[:4]:
            go(copy)

    def join_sums(k):
        copies = spread(k)
        copies[0].wait_recv()
        add_mate(k, xr, g0, xrelay[k, 0])
        go(copies[4])
        copies[1].wait_recv()
        add_mate(k, xl, g1, xrelay[k, 1])
        go(copies[5])

    def finish(k):
        for copy in spread(k)[2:]:
            copy.wait_recv()
        total = part[k, c, x].astype(F32) + precv[k, x].astype(F32)
        total = total + xfin[k, 0].astype(F32) + xfin[k, 1].astype(F32)
        out[k * PC:(k + 1) * PC, :] = total.astype(BF)

    plan = (
        (last_keys, 0), (send_stats, 0), (last_keys, 1), (send_stats, 1), (send_shares, 0),
        (last_keys, 2), (send_stats, 2), (send_shares, 1), (join_shares, 0), (send_shares, 2),
        (join_shares, 1), (merge, 0), (join_shares, 2), (send_sums, 0), (merge, 1), (join_sums, 0),
        (send_sums, 1), (merge, 2), (join_sums, 1), (send_sums, 2), (finish, 0), (join_sums, 2),
        (finish, 1), (finish, 2),
    )
    for f, k in plan:
        with scope(f"{f.__name__}{k}"):
            f(k)
    with scope("drain"):
        for copy in sent:
            copy.wait_send()


def tables():
    inverse = ROPE_BASE ** (-np.arange(HD // 2, dtype=np.float64) * 2.0 / HD)
    inverse = inverse.astype(np.float32).astype(np.float64)
    inverse = np.concatenate([inverse, inverse])
    place = np.arange(ROWS).reshape(2 * NX, NCH, PC).transpose(1, 0, 2).reshape(-1)
    local = place[:, None] * inverse[None, :]
    offset = (np.arange(NZ * NY) * ROWS)[:, None] * inverse[None, :]
    return [f(a).astype(np.float32) for a in (local, offset) for f in (np.cos, np.sin)]


DMA = pltpu.SemaphoreType.DMA


def per_device(
    tokens, norm_gain, w_query, w_key, w_value, w_outer, w_inner, w_signal,
    conv_taps, lambdas, head_gain, attend_proj, convolve_proj,
):
    rc, rs, oc, os_ = tables()
    v = pltpu.VMEM
    mixed, lse = pl.pallas_call(
        layer_kernel,
        out_shape=(
            jax.ShapeDtypeStruct((BLK, 2048), BF),
            jax.ShapeDtypeStruct((ROWS, 2), F32),
        ),
        in_specs=[vmem()] * 9 + [hbm()] * 8,
        out_specs=(vmem(), vmem()),
        scratch_shapes=[
            v((2 * NX, ROWS, 256), BF), v((CH, 2048), BF), v((6, 2048, 256), BF),
            v((256, 2048), BF), v((256, 2048), BF),
            v((ROWS + 8, 256), F32), v((ROWS, 256), F32), v((ROWS, 256), BF),
            v((NY, ROWS, VD), BF), v((NZ, ROWS, 2 * VD), BF),
            v((2, NY, ROWS, HD), F32), v((2, NY, ROWS, HD), F32), v((2, NY, ROWS, VD), F32),
            v((ROWS, HD), F32), v((NY, NCH, 8, CH), F32), v((NY, ROWS, VD), BF),
            v((2, NCH * HF, VD), BF), v((2, ROWS, VD), BF),
            v((NCH, 2, NX, PC, 2048), BF), v((NCH, NX, PC, 2048), BF),
            v((NCH, 2, PC // 2, 2048), BF), v((NCH, 2, PC, 2048), BF),
            DMA((8,)), DMA((2,)), DMA((NCH, 9)), DMA((NCH, 9)),
            DMA((NCH, 6)), DMA((NCH, 6)), DMA((NCH, 6)), DMA((NCH, 6)),
            DMA((NCH, 3)), DMA((NCH, 3)), DMA((NCH, 6)), DMA((NCH, 6)),
            DMA((NCH,)), DMA((NCH,)), DMA((NCH, 6)), DMA((NCH, 6)),
        ],
        compiler_params=pltpu.CompilerParams(
            collective_id=1, has_side_effects=True, vmem_limit_bytes=62 * 2 ** 20
        ),
        name="layer",
    )(
        tokens, norm_gain.reshape(1, -1), lambdas.reshape(1, 1), head_gain.reshape(1, -1), conv_taps,
        rc, rs, oc, os_, w_query, w_key, w_value, w_outer, w_inner, w_signal, attend_proj, convolve_proj,
    )
    return mixed, lse


def solution(mesh):
    return jax.shard_map(
        per_device,
        mesh=mesh,
        in_specs=(
            P("sp", "tp"), P(), P(None, "tp"), P(None, "tp"), P(None, "tp"), P(None, "tp"),
            P(None, "tp"), P(None, "tp"), P(None, "tp"), P("tp"), P(), P("tp", None), P("tp", None),
        ),
        out_specs=(P(("sp", "tp"), None), P("sp", "tp")),
        check_vma=False,
    )
```

time: 356 us -> 101 us (0.28); the launches traced: 351 us -> 100 us
  waiting for transfers between devices: 174 us -> 0 us
  Pallas kernels: 0 us -> 96.1 us
  matrix products: 90.9 us -> 0 us
  other arithmetic: 30.5 us -> 0 us
  local copies, waits for them, and re-layouts: 24.8 us -> 2.54 us
  between operations: 14.8 us -> 1.3 us
  loops' own time: 11.9 us -> 0 us
    all_gather x3 -> x0, waiting for transfers between devices: 122 us -> none  [the longest x1 54.6 us: per_device(): lax.all_gather(key_rows, 'sp', axis=0, tiled=True)]
    pallas_call x0 -> x1, Pallas kernels: none -> 96.1 us  [per_device(): pl.pallas_call(layer_kernel, out_shape=(jax.ShapeDtypeStruct((BLK, 2048),...]
    dot_general x33 -> x0, matrix products: 90.9 us -> none  [the longest x13 35.5 us: absorb(): jnp.einsum('hjqk,khe->hjqe', lifted.astype(jnp.bfloat16), values_here, pr...]
    reduce_scatter x1 -> x0, waiting for transfers between devices: 51.2 us -> none  [per_device(): lax.psum_scatter((jnp.dot(attended, attend_proj, preferred_element_type=j...]
    reduce_sum x15 -> x0, other arithmetic: 16.9 us -> none  [the longest x13 14.1 us: absorb(): weight_sum = factor * weight_sum + jnp.sum(lifted, axis=3)]
    unnamed x29 -> x3, local copies, waits for them, and re-layouts: 13.7 us -> 0.75 us
    another operation x17 -> x0, loops' own time: 11.9 us -> none  [the longest x1 10.9 us: make_fold(): lax.scan(one_shard, carry, jnp.arange(shard_count, dtype=jnp.int32))]
    dynamic_slice x16 -> x0, local copies, waits for them, and re-layouts: 9.79 us -> none  [make_fold(): lax.scan(one_shard, carry, jnp.arange(shard_count, dtype=jnp.int32))]
  transfers between devices with their start and end apart: 5 -> 0, of which waited for: 4 -> 0; matrix products, arithmetic and copies ran while one was open for 37% -> 0% of each run, Pallas kernels for 0% -> 0%
where the time goes in v2:
time: 101 us; the launch traced here: 100 us
  Pallas kernels  96.1 us (95%)
  local copies, waits for them, and re-layouts  2.54 us (3%)
  between operations  1.3 us (1%)
    pallas_call x1, Pallas kernels, per_device(): pl.pallas_call(layer_kernel, out_shape=(jax.ShapeDtypeStruct((BLK, 2048),...  96.1 us

profile of v2, /device:TPU:97, one launch (start us, length us, event | category | flops | bytes accessed | tf_op | source)
XLA Modules:
  0.0 100.0 jit_solution(3089001269034661234)
XLA Ops:
  1.3 96.1 %layer.1 = (bf16[96,2048]{1,0:T(8,128)(2,1)}, f32[768,2]{1,0:T(8,128)}) custom-call(bf16[768,256]{1,0:T(8,128)(2,1)} %tok.1, f32[1,2048]{1,0:T(1,128)} %bitcast.4, f32[1,1]{1,0:T(1,128)} %bitcast.3.lam, f32[1,256]{1,0:T(1,128)} %bitcast.5, bf16[3,256]{1,0:T(4,128)(2,1)} %taps.1, f32[768,128]{1,0:T(8,128)} %constant.8.clone.rc, f32[768,128]{1,0:T(8,128)} %constant.9.clone.rs, ...), custom_call_target="tpu_custom_call" | custom-call | tf_op jit(solution)/shard_map/layer/pallas_call | solution.py:521
  97.4 0.0 copy-start
  97.4 1.8 %copy.19 = f32[768,2]{0,1:T(2,128)} copy(f32[768,2]{1,0:T(8,128)} %get-tuple-element.3) | data formatting | bytes 12288 | tf_op jit(solution)/shard_map/layer/pallas_call | solution.py:521
  99.2 0.0 copy-done
  99.2 0.7 copy.22
Async XLA Ops:
  97.4 1.8 %copy-start = (bf16[96,2048]{1,0:T(8,128)(2,1)S(1)}, bf16[96,2048]{1,0:T(8,128)(2,1)}, u32[]{:S(2)}) copy-start(bf16[96,2048]{1,0:T(8,128)(2,1)} %get-tuple-element.6) | copy-start | bytes 1179652

commit v3 on v2

--- a/solution.py
+++ b/solution.py
@@ -54,12 +54,12 @@
 
 
 def layer_kernel(
-    tok, gain, lam, hgain, taps, rc, rs, oc, os_, wq, wk, wv, wo, wi, ws, ap, cp,
+    gain, lam, hgain, taps, oc, os_, tok, rch, rsh, wq, wk, wv, wo, wi, ws, ap, cp,
     out, lse_ref,
-    xbuf, sc, wbuf, apb, cpb, prod, outer, conv,
+    xbuf, gcol, rc, rs, wbuf, apb, cpb, prod, outer, conv, lnat, obuf,
     qb, kvb, m_ref, l_ref, acc, lt, stats, dbuf, relay, fin,
     part, precv, xrelay, xfin,
-    wsem, bsem, gss, grs, kss, krs, qss, qrs, tss, trs, dss, drs, pss, prs, xss, xrs,
+    wsem, tsem, osem, bsem, gss, grs, kss, krs, qss, qrs, tss, trs, dss, drs, pss, prs, xss, xrs,
 ):
     sp = lax.axis_index("sp")
     tp = lax.axis_index("tp")
@@ -74,14 +74,17 @@
     dn, dp = (lax.rem(sp + 1, NZ * NY), tp), (lax.rem(sp + NZ * NY - 1, NZ * NY), tp)
     right, left, opp = xr * 2 + c, xl * 2 + c, xo * 2 + c
 
+    tcopies = [
+        pltpu.make_async_copy(tok.at[:, pl.ds(k * PC, PC), :], xbuf.at[tp, k], tsem.at[k])
+        for k in range(NCH)
+    ]
+    for copy in tcopies:
+        copy.start()
     weights = ((wk, wbuf.at[0]), (wv, wbuf.at[1]), (wq, wbuf.at[2]), (wi, wbuf.at[3]),
-               (ws, wbuf.at[4]), (wo, wbuf.at[5]), (ap, apb), (cp, cpb))
+               (ws, wbuf.at[4]), (wo, wbuf.at[5]), (rch, rc), (rsh, rs), (ap, apb), (cp, cpb))
     wcopies = [pltpu.make_async_copy(a, b, wsem.at[i]) for i, (a, b) in enumerate(weights)]
     for copy in wcopies:
         copy.start()
-    for k in range(NCH):
-        for t in range(2 * NX):
-            xbuf[tp, k * CH + t * PC:k * CH + (t + 1) * PC, :] = tok[t * BLK + k * PC:t * BLK + (k + 1) * PC, :]
     with scope("greet"):
         greet([dxr, dxl, dm, dyr, dyl, dyo, dzr, dzl, dn, dp])
     sent = []
@@ -94,10 +97,11 @@
         return pl.ds(k * CH, CH) if h is None else pl.ds(k * CH + h * HF, HF)
 
     def pass_on(k, kind, block, h, dev):
-        ref = xbuf.at[block, rows_of(k, h)]
+        ref = xbuf.at[block, k] if h is None else xbuf.at[block, k, pl.ds(h * NX, NX)]
         return remote(ref, ref, gss.at[k, kind], grs.at[k, kind], dev)
 
     def send_own(k):
+        tcopies[k].wait()
         go(pass_on(k, 0, tp, None, dxr))
         go(pass_on(k, 1, tp, None, dxl))
         go(pass_on(k, 2, tp, None, dm))
@@ -152,6 +156,10 @@
             copies[1].wait_recv()
             copies[3].wait_recv()
 
+    def ring_right(rings):
+        for copies in rings:
+            copies[3].wait_recv()
+
     def ring_far(rings):
         for copies in rings:
             copies[4].wait_recv()
@@ -163,10 +171,11 @@
     def compute(k):
         rows = rows_of(k)
         square = jnp.zeros((CH, HD), F32)
-        for b in range(2 * NX):
-            xb = xbuf[b, rows, :].astype(F32)
-            square += xb[:, :HD] * xb[:, :HD] + xb[:, HD:] * xb[:, HD:]
-            sc[:, b * 256:(b + 1) * 256] = (xb * gain[:, b * 256:(b + 1) * 256]).astype(BF)
+        blocks = [xbuf[b, k].reshape(CH, 256) for b in range(2 * NX)]
+        for xb in blocks:
+            xf = xb.astype(F32)
+            square += xf[:, :HD] * xf[:, :HD] + xf[:, HD:] * xf[:, HD:]
+        wide = jnp.concatenate(blocks, axis=1)
         total = jnp.sum(square, axis=1, keepdims=True)
         inv = lax.rsqrt(total / (2 * NX * 256) + NORM_EPS)
         c_r, s_r = rc[rows, :], rs[rows, :]
@@ -176,7 +185,7 @@
         sine = jnp.where(lane < HD // 2, -sine, sine)
 
         def project(i):
-            return inv * jnp.dot(sc[...], wbuf[i], preferred_element_type=F32)
+            return inv * jnp.dot(wide, wbuf[i], preferred_element_type=F32)
 
         def turn(v):
             parts = []
@@ -231,6 +240,22 @@
         col = place(lax.broadcasted_iota(jnp.int32, (1, ROWS), 1))
         attend(y, z, pl.ds(0, ROWS), col <= row)
 
+    def scale_weights():
+        g = jnp.concatenate([gain[...], jnp.zeros((HD - 16, HD), F32)], axis=0)
+        g = jnp.transpose(g)
+        for b in range(16):
+            gcol[b * HD:(b + 1) * HD, :] = jnp.broadcast_to(g[:, b:b + 1], (HD, HD))
+
+        def one(i, _):
+            for b in range(8):
+                rows = slice(b * 256, (b + 1) * 256)
+                col = gcol[rows, :]
+                w = wbuf[i, rows, :].astype(F32)
+                wbuf[i, rows, :] = (w * jnp.concatenate([col, col], axis=1)).astype(BF)
+            return 0
+
+        lax.fori_loop(0, 6, one, 0)
+
     def start():
         m_ref[...] = jnp.full(m_ref.shape, MASKED, F32)
         l_ref[...] = jnp.zeros(l_ref.shape, F32)
@@ -238,7 +263,12 @@
 
     send_own(0)
     send_own(1)
-    start()
+    with scope("init"):
+        start()
+        for copy in wcopies:
+            copy.wait()
+    with scope("scale"):
+        scale_weights()
     with scope("near0"):
         near(0)
     with scope("near1"):
@@ -248,8 +278,6 @@
         far(0)
     with scope("mates0"):
         mates(0)
-        for copy in wcopies:
-            copy.wait()
     with scope("comp0"):
         compute(0)
     with scope("near2"):
@@ -302,14 +330,14 @@
         @pl.when(i == 3)
         def _():
             with scope("krest"):
-                ring_rest(kring)
+                for copies in kring:
+                    copies[1].wait_recv()
 
         mine = i < 3
-        first = i < 7
         turn_ = jnp.where(i == 0, 1, jnp.where(i == 1, 3, 2))
         qi = jnp.where(mine, lax.rem(y + turn_, NY), lax.rem(i + 1, NY))
-        kj = jnp.where(mine, z, jnp.where(first, zl, zr))
-        need = (mine & (qi > y)) | (~mine & first & (z >= 1)) | (~first & (z == 3))
+        kj = jnp.where(mine, z, zl)
+        need = (mine & (qi > y)) | (~mine & (z >= 1))
 
         @pl.when(need)
         def _():
@@ -325,21 +353,45 @@
         copies[2].wait_recv()
         copies[5].start()
 
-    lax.fori_loop(0, 11, step, 0)
+    lax.fori_loop(0, 7, step, 0)
     sent.append(kring[2][4])
     sent.append(kring[2][5])
-    with scope("kfar"):
-        ring_far(kring)
-
-    lam_v = lam[...]
-
-    def last_keys(k):
-        @pl.when(z >= 2)
-        def _():
-            ss = [[scores(qi, zo, rows_of(k), j) for qi in range(NY)] for j in range(2)]
-            for j in range(2):
-                for qi in range(NY):
-                    absorb(qi, zo, rows_of(k), j, ss[j][qi])
+    lam_v = lam[0]
+
+    def last_keys(k, between):
+        def body(i, _):
+            right_turn = i == 0
+            if k == 0:
+                @pl.when(right_turn)
+                def _():
+                    with scope("kright"):
+                        ring_right(kring)
+
+                @pl.when(i == 1)
+                def _():
+                    with scope("kfar"):
+                        ring_far(kring)
+
+            kj = jnp.where(right_turn, zr, zo)
+
+            @pl.when((z == 3) | ((i == 1) & (z == 2)))
+            def _():
+                with scope("tiles"):
+                    ss = [[scores(qi, kj, rows_of(k), j) for qi in range(NY)] for j in range(2)]
+                    for j in range(2):
+                        for qi in range(NY):
+                            absorb(qi, kj, rows_of(k), j, ss[j][qi])
+
+            if between:
+                @pl.when(right_turn)
+                def _():
+                    for f, kk in between:
+                        with scope(f"{f.__name__}{kk}"):
+                            f(kk)
+
+            return 0
+
+        lax.fori_loop(0, 2, body, 0)
 
     def stat_copies(k):
         ref = stats.at[y, k]
@@ -358,7 +410,7 @@
                 table = jnp.where(lane == 2 * qi + j, lse, table)
         stats[y, k] = jnp.transpose(table)[0:8, :]
         for copy in stat_copies(k):
-            go(copy)
+            copy.start()
 
     def pick(rows, qi, j):
         lanes = lax.broadcasted_iota(jnp.int32, (CH, HD), 1)
@@ -400,7 +452,7 @@
 
         lax.fori_loop(0, NY - 1, one, 0)
         for copy in scatter(k)[:4]:
-            go(copy)
+            copy.start()
 
     def join_shares(k):
         copies = scatter(k)
@@ -408,10 +460,10 @@
         at = pl.ds(k * HF, HF)
         copies[0].wait_recv()
         dbuf[yr, h0, :] = (dbuf[yr, h0, :].astype(F32) + relay[0, at, :].astype(F32)).astype(BF)
-        go(copies[4])
+        copies[4].start()
         copies[1].wait_recv()
         dbuf[yl, h1, :] = (dbuf[yl, h1, :].astype(F32) + relay[1, at, :].astype(F32)).astype(BF)
-        go(copies[5])
+        copies[5].start()
 
     def mate_copy(k):
         return remote(part.at[k, 1 - c], precv.at[k], pss.at[k], prs.at[k], dm)
@@ -423,11 +475,9 @@
         d = share(rows, y) + fin[0, rows, :].astype(F32) + fin[1, rows, :].astype(F32)
         back = lax.rsqrt(jnp.mean(d * d, axis=1, keepdims=True) + NORM_EPS)
         att = (d * back * hgain[...] * HEAD_KEEP).astype(BF)
-        ls = [pick(rows, y, j) * LN2 for j in range(2)]
         pieces = [slice(t * BLK + k * PC, t * BLK + (k + 1) * PC) for t in range(2 * NX)]
         for t in range(2 * NX):
-            for j in range(2):
-                lse_ref[pieces[t], j:j + 1] = ls[j][t * PC:(t + 1) * PC]
+            lnat[pieces[t], :] = lt[k * CH + t * PC:k * CH + (t + 1) * PC, :]
         con = jnp.concatenate([conv[pieces[t], :] for t in range(2 * NX)], axis=0)
         cols = 512
         for n in range(2048 // cols):
@@ -438,7 +488,7 @@
             p = p.astype(BF)
             for t in range(2 * NX):
                 part[k, t % 2, t // 2, :, cs] = p[t * PC:(t + 1) * PC]
-        go(mate_copy(k))
+        mate_copy(k).start()
 
     g0, g1 = pl.ds(0, PC // 2), pl.ds(PC // 2, PC // 2)
 
@@ -466,35 +516,55 @@
         add_mate(k, xr, g1)
         add_mate(k, xl, g0)
         for copy in copies[:4]:
-            go(copy)
+            copy.start()
 
     def join_sums(k):
         copies = spread(k)
         copies[0].wait_recv()
         add_mate(k, xr, g0, xrelay[k, 0])
-        go(copies[4])
+        copies[4].start()
         copies[1].wait_recv()
         add_mate(k, xl, g1, xrelay[k, 1])
-        go(copies[5])
+        copies[5].start()
 
     def finish(k):
         for copy in spread(k)[2:]:
             copy.wait_recv()
         total = part[k, c, x].astype(F32) + precv[k, x].astype(F32)
         total = total + xfin[k, 0].astype(F32) + xfin[k, 1].astype(F32)
-        out[k * PC:(k + 1) * PC, :] = total.astype(BF)
-
-    plan = (
-        (last_keys, 0), (send_stats, 0), (last_keys, 1), (send_stats, 1), (send_shares, 0),
-        (last_keys, 2), (send_stats, 2), (send_shares, 1), (join_shares, 0), (send_shares, 2),
-        (join_shares, 1), (merge, 0), (join_shares, 2), (send_sums, 0), (merge, 1), (join_sums, 0),
-        (send_sums, 1), (merge, 2), (join_sums, 1), (send_sums, 2), (finish, 0), (join_sums, 2),
-        (finish, 1), (finish, 2),
-    )
-    for f, k in plan:
-        with scope(f"{f.__name__}{k}"):
-            f(k)
+        obuf[k] = total.astype(BF)
+        out_copy(k).start()
+
+    def out_copy(k):
+        return pltpu.make_async_copy(obuf.at[k], out.at[pl.ds(k * PC, PC)], osem.at[k])
+
+    def row_lse(k):
+        flat = jnp.transpose(lnat[...])
+        mine = jnp.zeros((2, ROWS), F32)
+        for i in range(NY):
+            mine = jnp.where(y == i, flat[2 * i:2 * i + 2, :], mine)
+        lse_ref[...] = mine * LN2
+
+    def run(plan):
+        for f, k in plan:
+            with scope(f"{f.__name__}{k}"):
+                f(k)
+
+    last_keys(0, ())
+    run(((send_stats, 0),))
+    last_keys(1, ((send_shares, 0),))
+    run(((send_stats, 1), (join_shares, 0)))
+    last_keys(2, ((send_shares, 1), (merge, 0)))
+    run((
+        (send_stats, 2), (join_shares, 1), (send_sums, 0), (send_shares, 2), (merge, 1),
+        (join_sums, 0), (send_sums, 1), (join_shares, 2), (merge, 2), (join_sums, 1),
+        (send_sums, 2), (finish, 0), (row_lse, 0), (join_sums, 2), (finish, 1), (finish, 2),
+    ))
     with scope("drain"):
+        for k in range(NCH):
+            out_copy(k).wait()
+            for copy in stat_copies(k) + scatter(k) + [mate_copy(k)] + spread(k):
+                copy.wait_send()
         for copy in sent:
             copy.wait_send()
 
@@ -522,21 +592,23 @@
         layer_kernel,
         out_shape=(
             jax.ShapeDtypeStruct((BLK, 2048), BF),
-            jax.ShapeDtypeStruct((ROWS, 2), F32),
+            jax.ShapeDtypeStruct((2, ROWS), F32),
         ),
-        in_specs=[vmem()] * 9 + [hbm()] * 8,
-        out_specs=(vmem(), vmem()),
+        in_specs=[vmem(), pl.BlockSpec(memory_space=pltpu.SMEM)] + [vmem()] * 4 + [hbm()] * 11,
+        out_specs=(hbm(), vmem()),
         scratch_shapes=[
-            v((2 * NX, ROWS, 256), BF), v((CH, 2048), BF), v((6, 2048, 256), BF),
+            v((2 * NX, NCH, 2 * NX, PC, 256), BF), v((2048, HD), F32), v((ROWS, HD), F32), v((ROWS, HD), F32),
+            v((6, 2048, 256), BF),
             v((256, 2048), BF), v((256, 2048), BF),
-            v((ROWS + 8, 256), F32), v((ROWS, 256), F32), v((ROWS, 256), BF),
+            v((ROWS + 8, 256), F32), v((ROWS, 256), F32), v((ROWS, 256), BF), v((ROWS, HD), F32),
+            v((NCH, PC, 2048), BF),
             v((NY, ROWS, VD), BF), v((NZ, ROWS, 2 * VD), BF),
             v((2, NY, ROWS, HD), F32), v((2, NY, ROWS, HD), F32), v((2, NY, ROWS, VD), F32),
             v((ROWS, HD), F32), v((NY, NCH, 8, CH), F32), v((NY, ROWS, VD), BF),
             v((2, NCH * HF, VD), BF), v((2, ROWS, VD), BF),
             v((NCH, 2, NX, PC, 2048), BF), v((NCH, NX, PC, 2048), BF),
             v((NCH, 2, PC // 2, 2048), BF), v((NCH, 2, PC, 2048), BF),
-            DMA((8,)), DMA((2,)), DMA((NCH, 9)), DMA((NCH, 9)),
+            DMA((10,)), DMA((NCH,)), DMA((NCH,)), DMA((2,)), DMA((NCH, 9)), DMA((NCH, 9)),
             DMA((NCH, 6)), DMA((NCH, 6)), DMA((NCH, 6)), DMA((NCH, 6)),
             DMA((NCH, 3)), DMA((NCH, 3)), DMA((NCH, 6)), DMA((NCH, 6)),
             DMA((NCH,)), DMA((NCH,)), DMA((NCH, 6)), DMA((NCH, 6)),
@@ -546,10 +618,11 @@
         ),
         name="layer",
     )(
-        tokens, norm_gain.reshape(1, -1), lambdas.reshape(1, 1), head_gain.reshape(1, -1), conv_taps,
-        rc, rs, oc, os_, w_query, w_key, w_value, w_outer, w_inner, w_signal, attend_proj, convolve_proj,
+        norm_gain.reshape(16, HD), lambdas, head_gain.reshape(1, -1), conv_taps, oc, os_,
+        tokens.reshape(2 * NX, BLK, 256), rc, rs,
+        w_query, w_key, w_value, w_outer, w_inner, w_signal, attend_proj, convolve_proj,
     )
-    return mixed, lse
+    return mixed, lse.T
 
 
 def solution(mesh):

time: 101 us -> 98 us (0.970)
  Pallas kernels: 96.1 us -> 94.2 us
    pallas_call x1, Pallas kernels: 96.1 us -> 94.2 us  [per_device(): pl.pallas_call(layer_kernel, out_shape=(jax.ShapeDtypeStruct((BLK, 2048),...]
    pallas_call x1 -> x0, local copies, waits for them, and re-layouts: 1.79 us -> none  [per_device(): pl.pallas_call(layer_kernel, out_shape=(jax.ShapeDtypeStruct((BLK, 2048),...]
    unnamed x3 -> x4, local copies, waits for them, and re-layouts: 0.75 us -> 2.37 us
where the time goes in v3:
time: 98 us; the launch traced here: 97.8 us
  Pallas kernels  94.2 us (96%)
  local copies, waits for them, and re-layouts  2.37 us (2%)
  between operations  1.3 us (1%)
    pallas_call x1, Pallas kernels, per_device(): pl.pallas_call(layer_kernel, out_shape=(jax.ShapeDtypeStruct((BLK, 2048),...  94.2 us
    unnamed x4, local copies, waits for them, and re-layouts  2.37 us

profile of v3, /device:TPU:97, one launch (start us, length us, event | category | flops | bytes accessed | tf_op | source)
XLA Modules:
  0.0 97.8 jit_solution(14160774451403476229)
XLA Ops:
  1.3 94.2 %layer.1 = (bf16[96,2048]{1,0:T(8,128)(2,1)}, f32[2,768]{1,0:T(2,128)}) custom-call(f32[16,128]{1,0:T(8,128)} %bitcast.5, f32[1]{0:T(128)S(6)} %copy.21.lam, f32[1,256]{1,0:T(1,128)} %bitcast.7, bf16[3,256]{1,0:T(4,128)(2,1)} %taps.1, f32[16,128]{1,0:T(8,128)} %constant.8.clone.oc, f32[16,128]{1,0:T(8,128)} %constant.9.clone.os_, ...), custom_call_target="tpu_custom_call" | custom-call | tf_op jit(solution)/shard_map/layer/pallas_call | solution.py:591
  95.5 0.0 copy-start
  95.5 1.8 %copy.22 = bf16[96,2048]{1,0:T(8,128)(2,1)} copy(bf16[96,2048]{1,0:T(8,128)(2,1)} %get-tuple-element.8) | data formatting | bytes 786432
  97.2 0.0 copy-done
  97.2 0.6 copy.23
Async XLA Ops:
  95.5 1.8 %copy-start = (f32[2,768]{1,0:T(2,128)S(1)}, f32[2,768]{1,0:T(2,128)}, u32[]{:S(2)}) copy-start(f32[2,768]{1,0:T(2,128)} %get-tuple-element.5) | copy-start | bytes 18436

commit v4 on v3

--- a/solution.py
+++ b/solution.py
@@ -56,10 +56,10 @@
 def layer_kernel(
     gain, lam, hgain, taps, oc, os_, tok, rch, rsh, wq, wk, wv, wo, wi, ws, ap, cp,
     out, lse_ref,
-    xbuf, gcol, rc, rs, wbuf, apb, cpb, prod, outer, conv, lnat, obuf,
+    xbuf, gcol, rc, rs, wbuf, apb, cpb, prod, outer, conv, lnat,
     qb, kvb, m_ref, l_ref, acc, lt, stats, dbuf, relay, fin,
     part, precv, xrelay, xfin,
-    wsem, tsem, osem, bsem, gss, grs, kss, krs, qss, qrs, tss, trs, dss, drs, pss, prs, xss, xrs,
+    wsem, tsem, bsem, send, grs, krs, qrs, trs, drs, prs, xrs,
 ):
     sp = lax.axis_index("sp")
     tp = lax.axis_index("tp")
@@ -87,18 +87,17 @@
         copy.start()
     with scope("greet"):
         greet([dxr, dxl, dm, dyr, dyl, dyo, dzr, dzl, dn, dp])
-    sent = []
 
     def go(copy):
         copy.start()
-        sent.append(copy)
 
     def rows_of(k, h=None):
         return pl.ds(k * CH, CH) if h is None else pl.ds(k * CH + h * HF, HF)
 
     def pass_on(k, kind, block, h, dev):
+        slot = (0, 1, 4, 2, 3, 4, 4, 4, 4)[kind]
         ref = xbuf.at[block, k] if h is None else xbuf.at[block, k, pl.ds(h * NX, NX)]
-        return remote(ref, ref, gss.at[k, kind], grs.at[k, kind], dev)
+        return remote(ref, ref, send.at[0], grs.at[k, slot], dev)
 
     def send_own(k):
         tcopies[k].wait()
@@ -121,49 +120,35 @@
         go(pass_on(k, 8, opp, 1, dm))
 
     def mates(k):
-        pass_on(k, 2, tp, None, dm).wait_recv()
-        pass_on(k, 5, left, None, dm).wait_recv()
-        pass_on(k, 6, right, None, dm).wait_recv()
-        pass_on(k, 7, opp, 0, dm).wait_recv()
-        pass_on(k, 8, opp, 1, dm).wait_recv()
+        ref = xbuf.at[pl.ds(0, NX), k]
+        remote(ref, ref, send.at[0], grs.at[k, 4], dm).wait_recv()
 
     def ring(buf, me, lf, rt, ss, rs_, d_r, d_l):
         def one(block, k, h, kind, dev):
             ref = buf.at[block, rows_of(k, h)]
-            return remote(ref, ref, ss.at[k, kind], rs_.at[k, kind], dev)
+            return remote(ref, ref, ss, rs_.at[kind if kind == 6 else 2 * k + kind], dev)
 
         return [
-            [one(me, k, 0, 0, d_r), one(me, k, 1, 1, d_r), one(me, k, 1, 2, d_l),
-             one(me, k, 0, 3, d_l), one(lf, k, 0, 4, d_r), one(rt, k, 1, 5, d_l)]
+            [one(me, k, None, 0, d_r), one(me, k, None, 1, d_l),
+             one(lf, k, 0, 6, d_r), one(rt, k, 1, 6, d_l)]
             for k in range(NCH)
         ]
 
-    kring = ring(kvb, z, zl, zr, kss, krs, dzr, dzl)
-    qring = ring(qb, y, yl, yr, qss, qrs, dyr, dyl)
+    kring = ring(kvb, z, zl, zr, send.at[1], krs, dzr, dzl)
+    qring = ring(qb, y, yl, yr, send.at[2], qrs, dyr, dyl)
 
     def ring_send(copies):
-        for i in (0, 2, 1, 3):
-            go(copies[i])
+        copies[0].start()
+        copies[1].start()
 
     def ring_relay(copies):
         copies[0].wait_recv()
-        go(copies[4])
-        copies[2].wait_recv()
-        go(copies[5])
-
-    def ring_rest(rings):
-        for copies in rings:
-            copies[1].wait_recv()
-            copies[3].wait_recv()
-
-    def ring_right(rings):
-        for copies in rings:
-            copies[3].wait_recv()
-
-    def ring_far(rings):
-        for copies in rings:
-            copies[4].wait_recv()
-            copies[5].wait_recv()
+        copies[2].start()
+        copies[1].wait_recv()
+        copies[3].start()
+
+    def ring_far(buf, sem, me, dev):
+        remote(buf.at[me], buf.at[me], send.at[1], sem.at[6], dev).wait_recv()
 
     co = oc[pl.ds(sp, 1), :]
     so = os_[pl.ds(sp, 1), :]
@@ -197,14 +182,14 @@
         kvb[z, rows, 0:VD] = turn(project(0)).astype(BF)
         kvb[z, rows, VD:2 * VD] = project(1).astype(BF)
         qb[y, rows, :] = (turn(project(2)) * (LOG2E * HD ** -0.5)).astype(BF)
-        ring_send(kring[k])
-        ring_send(qring[k])
         pr = project(3) * project(4)
         og = project(5)
         for t in range(2 * NX):
             at = t * BLK + k * PC
             prod[8 + at:8 + at + PC, :] = pr[t * PC:(t + 1) * PC]
             outer[at:at + PC, :] = og[t * PC:(t + 1) * PC]
+        ring_send(kring[k])
+        ring_send(qring[k])
 
     def scores(qi, kj, rows, j):
         q = qb[qi, rows, j * HD:(j + 1) * HD]
@@ -276,34 +261,33 @@
     send_own(2)
     with scope("far0"):
         far(0)
+    with scope("near2"):
+        near(2)
     with scope("mates0"):
         mates(0)
     with scope("comp0"):
         compute(0)
-    with scope("near2"):
-        near(2)
     with scope("far1"):
         far(1)
+    with scope("far2"):
+        far(2)
+    with scope("mates1"):
         mates(1)
     with scope("comp1"):
         compute(1)
-    with scope("far2"):
-        far(2)
+    with scope("mates2"):
         mates(2)
     with scope("qrel0"):
         ring_relay(qring[0])
     with scope("comp2"):
         compute(2)
     border = remote(prod.at[pl.ds(ROWS, 8)], prod.at[pl.ds(0, 8)], bsem.at[0], bsem.at[1], dn)
-    go(border)
+    border.start()
+    with scope("own"):
+        own_pair()
     with scope("rel0"):
         ring_relay(kring[0])
         ring_relay(qring[1])
-    with scope("own"):
-        own_pair()
-    with scope("rel1"):
-        ring_relay(kring[1])
-        ring_relay(qring[2])
     with scope("conv"):
         border.wait_recv()
 
@@ -316,22 +300,21 @@
             tv[0:1] * prod[6:6 + ROWS, :] + tv[1:2] * prod[7:7 + ROWS, :] + tv[2:3] * prod[8:8 + ROWS, :]
         )
         conv[...] = (outer[...] * smoothed).astype(BF)
-    with scope("qrest"):
-        ring_rest(qring)
+    with scope("qrel2"):
+        ring_relay(qring[2])
+    with scope("rel1"):
+        ring_relay(kring[1])
 
     def step(i, _):
         @pl.when(i == 2)
         def _():
             with scope("qfar"):
-                ring_far(qring)
-            with scope("rel2"):
-                ring_relay2()
+                ring_far(qb, qrs, y, dyr)
 
         @pl.when(i == 3)
         def _():
-            with scope("krest"):
-                for copies in kring:
-                    copies[1].wait_recv()
+            with scope("rel2"):
+                ring_relay(kring[2])
 
         mine = i < 3
         turn_ = jnp.where(i == 0, 1, jnp.where(i == 1, 3, 2))
@@ -346,31 +329,17 @@
 
         return 0
 
-    def ring_relay2():
-        copies = kring[2]
-        copies[0].wait_recv()
-        copies[4].start()
-        copies[2].wait_recv()
-        copies[5].start()
-
     lax.fori_loop(0, 7, step, 0)
-    sent.append(kring[2][4])
-    sent.append(kring[2][5])
     lam_v = lam[0]
 
     def last_keys(k, between):
         def body(i, _):
             right_turn = i == 0
             if k == 0:
-                @pl.when(right_turn)
-                def _():
-                    with scope("kright"):
-                        ring_right(kring)
-
                 @pl.when(i == 1)
                 def _():
                     with scope("kfar"):
-                        ring_far(kring)
+                        ring_far(kvb, krs, z, dzr)
 
             kj = jnp.where(right_turn, zr, zo)
 
@@ -396,7 +365,7 @@
     def stat_copies(k):
         ref = stats.at[y, k]
         return [
-            remote(ref, ref, tss.at[k, i], trs.at[k, i], dev) for i, dev in enumerate((dyr, dyl, dyo))
+            remote(ref, ref, send.at[3], trs.at[k], dev) for dev in (dyr, dyl, dyo)
         ]
 
     def send_stats(k):
@@ -434,12 +403,14 @@
             (dbuf.at[yr, h0], fin.at[0, h0], dyr),
             (dbuf.at[yl, h1], fin.at[1, h1], dyl),
         ]
-        return [remote(a, b, dss.at[k, i], drs.at[k, i], d) for i, (a, b, d) in enumerate(pairs)]
+        return [
+            remote(a, b, send.at[4], drs.at[k, min(i, 2)], d) for i, (a, b, d) in enumerate(pairs)
+        ]
 
     def send_shares(k):
         rows = rows_of(k)
-        for copy in stat_copies(k):
-            copy.wait_recv()
+        ref = stats.at[pl.ds(0, NY - 1), k]
+        remote(ref, ref, send.at[3], trs.at[k], dyr).wait_recv()
         parts = [stats[i, k] for i in range(NY)]
         peak = jnp.maximum(jnp.maximum(parts[0], parts[1]), jnp.maximum(parts[2], parts[3]))
         whole = peak + jnp.log2(sum(jnp.exp2(p - peak) for p in parts))
@@ -466,12 +437,12 @@
         copies[5].start()
 
     def mate_copy(k):
-        return remote(part.at[k, 1 - c], precv.at[k], pss.at[k], prs.at[k], dm)
+        return remote(part.at[k, 1 - c], precv.at[k], send.at[5], prs.at[k], dm)
 
     def merge(k):
         rows = rows_of(k)
-        for copy in scatter(k)[2:]:
-            copy.wait_recv()
+        ref = fin.at[:, rows]
+        remote(ref, ref, send.at[4], drs.at[k, 2], dyr).wait_recv()
         d = share(rows, y) + fin[0, rows, :].astype(F32) + fin[1, rows, :].astype(F32)
         back = lax.rsqrt(jnp.mean(d * d, axis=1, keepdims=True) + NORM_EPS)
         att = (d * back * hgain[...] * HEAD_KEEP).astype(BF)
@@ -501,7 +472,9 @@
             (part.at[k, c, xr, g0], xfin.at[k, 0, g0], dxr),
             (part.at[k, c, xl, g1], xfin.at[k, 1, g1], dxl),
         ]
-        return [remote(a, b, xss.at[k, i], xrs.at[k, i], d) for i, (a, b, d) in enumerate(pairs)]
+        return [
+            remote(a, b, send.at[6], xrs.at[k, min(i, 2)], d) for i, (a, b, d) in enumerate(pairs)
+        ]
 
     def add_mate(k, xx, g, extra=None):
         t = part[k, c, xx, g, :].astype(F32) + precv[k, xx, g, :].astype(F32)
@@ -528,15 +501,10 @@
         copies[5].start()
 
     def finish(k):
-        for copy in spread(k)[2:]:
-            copy.wait_recv()
+        remote(xfin.at[k], xfin.at[k], send.at[6], xrs.at[k, 2], dxr).wait_recv()
         total = part[k, c, x].astype(F32) + precv[k, x].astype(F32)
         total = total + xfin[k, 0].astype(F32) + xfin[k, 1].astype(F32)
-        obuf[k] = total.astype(BF)
-        out_copy(k).start()
-
-    def out_copy(k):
-        return pltpu.make_async_copy(obuf.at[k], out.at[pl.ds(k * PC, PC)], osem.at[k])
+        out[k * PC:(k + 1) * PC, :] = total.astype(BF)
 
     def row_lse(k):
         flat = jnp.transpose(lnat[...])
@@ -561,12 +529,11 @@
         (send_sums, 2), (finish, 0), (row_lse, 0), (join_sums, 2), (finish, 1), (finish, 2),
     ))
     with scope("drain"):
-        for k in range(NCH):
-            out_copy(k).wait()
-            for copy in stat_copies(k) + scatter(k) + [mate_copy(k)] + spread(k):
-                copy.wait_send()
-        for copy in sent:
-            copy.wait_send()
+        groups = (xbuf.at[pl.ds(0, 7)], kvb.at[pl.ds(0, 3)], qb.at[pl.ds(0, 3)],
+                  stats.at[pl.ds(0, 3)], dbuf.at[pl.ds(0, 3)], precv, part.at[:, 0, pl.ds(0, 3)])
+        for i, ref in enumerate(groups):
+            remote(ref, ref, send.at[i], grs.at[0, 0], dm).wait_send()
+        border.wait_send()
 
 
 def tables():
@@ -595,23 +562,20 @@
             jax.ShapeDtypeStruct((2, ROWS), F32),
         ),
         in_specs=[vmem(), pl.BlockSpec(memory_space=pltpu.SMEM)] + [vmem()] * 4 + [hbm()] * 11,
-        out_specs=(hbm(), vmem()),
+        out_specs=(vmem(), vmem()),
         scratch_shapes=[
             v((2 * NX, NCH, 2 * NX, PC, 256), BF), v((2048, HD), F32), v((ROWS, HD), F32), v((ROWS, HD), F32),
             v((6, 2048, 256), BF),
             v((256, 2048), BF), v((256, 2048), BF),
             v((ROWS + 8, 256), F32), v((ROWS, 256), F32), v((ROWS, 256), BF), v((ROWS, HD), F32),
-            v((NCH, PC, 2048), BF),
             v((NY, ROWS, VD), BF), v((NZ, ROWS, 2 * VD), BF),
             v((2, NY, ROWS, HD), F32), v((2, NY, ROWS, HD), F32), v((2, NY, ROWS, VD), F32),
             v((ROWS, HD), F32), v((NY, NCH, 8, CH), F32), v((NY, ROWS, VD), BF),
             v((2, NCH * HF, VD), BF), v((2, ROWS, VD), BF),
             v((NCH, 2, NX, PC, 2048), BF), v((NCH, NX, PC, 2048), BF),
             v((NCH, 2, PC // 2, 2048), BF), v((NCH, 2, PC, 2048), BF),
-            DMA((10,)), DMA((NCH,)), DMA((NCH,)), DMA((2,)), DMA((NCH, 9)), DMA((NCH, 9)),
-            DMA((NCH, 6)), DMA((NCH, 6)), DMA((NCH, 6)), DMA((NCH, 6)),
-            DMA((NCH, 3)), DMA((NCH, 3)), DMA((NCH, 6)), DMA((NCH, 6)),
-            DMA((NCH,)), DMA((NCH,)), DMA((NCH, 6)), DMA((NCH, 6)),
+            DMA((10,)), DMA((NCH,)), DMA((2,)), DMA((7,)), DMA((NCH, 5)), DMA((7,)), DMA((7,)),
+            DMA((NCH,)), DMA((NCH, 3)), DMA((NCH,)), DMA((NCH, 3)),
         ],
         compiler_params=pltpu.CompilerParams(
             collective_id=1, has_side_effects=True, vmem_limit_bytes=62 * 2 ** 20

time: 98 us -> 99.3 us (1.013)
  Pallas kernels: 94.2 us -> 95.3 us
    pallas_call x1, Pallas kernels: 94.2 us -> 95.3 us  [per_device(): pl.pallas_call(layer_kernel, out_shape=(jax.ShapeDtypeStruct((BLK, 2048),...]
where the time goes in v4:
time: 99.3 us; the launch traced here: 99 us
  Pallas kernels  95.3 us (96%)
  local copies, waits for them, and re-layouts  2.37 us (2%)
  between operations  1.3 us (1%)
    pallas_call x1, Pallas kernels, per_device(): pl.pallas_call(layer_kernel, out_shape=(jax.ShapeDtypeStruct((BLK, 2048),...  95.3 us
    unnamed x4, local copies, waits for them, and re-layouts  2.37 us

profile of v4, /device:TPU:97, one launch (start us, length us, event | category | flops | bytes accessed | tf_op | source)
XLA Modules:
  0.0 99.0 jit_solution(8004145319285515963)
XLA Ops:
  1.3 95.3 %layer.1 = (bf16[96,2048]{1,0:T(8,128)(2,1)}, f32[2,768]{1,0:T(2,128)}) custom-call(f32[16,128]{1,0:T(8,128)} %bitcast.5, f32[1]{0:T(128)S(6)} %copy.21.lam, f32[1,256]{1,0:T(1,128)} %bitcast.7, bf16[3,256]{1,0:T(4,128)(2,1)} %taps.1, f32[16,128]{1,0:T(8,128)} %constant.8.clone.oc, f32[16,128]{1,0:T(8,128)} %constant.9.clone.os_, ...), custom_call_target="tpu_custom_call" | custom-call | tf_op jit(solution)/shard_map/layer/pallas_call | solution.py:558
  96.6 0.0 copy-start
  96.6 1.8 %copy.22 = bf16[96,2048]{1,0:T(8,128)(2,1)} copy(bf16[96,2048]{1,0:T(8,128)(2,1)} %get-tuple-element.8) | data formatting | bytes 786432
  98.4 0.0 copy-done
  98.4 0.6 copy.23
Async XLA Ops:
  96.6 1.8 %copy-start = (f32[2,768]{1,0:T(2,128)S(1)}, f32[2,768]{1,0:T(2,128)}, u32[]{:S(2)}) copy-start(f32[2,768]{1,0:T(2,128)} %get-tuple-element.5) | copy-start | bytes 18436

commit v5 on v4

--- a/solution.py
+++ b/solution.py
@@ -150,6 +150,7 @@
     def ring_far(buf, sem, me, dev):
         remote(buf.at[me], buf.at[me], send.at[1], sem.at[6], dev).wait_recv()
 
+    border = remote(prod.at[pl.ds(ROWS, 8)], prod.at[pl.ds(0, 8)], bsem.at[0], bsem.at[1], dn)
     co = oc[pl.ds(sp, 1), :]
     so = os_[pl.ds(sp, 1), :]
 
@@ -188,6 +189,8 @@
             at = t * BLK + k * PC
             prod[8 + at:8 + at + PC, :] = pr[t * PC:(t + 1) * PC]
             outer[at:at + PC, :] = og[t * PC:(t + 1) * PC]
+        if k == NCH - 1:
+            border.start()
         ring_send(kring[k])
         ring_send(qring[k])
 
@@ -261,33 +264,28 @@
     send_own(2)
     with scope("far0"):
         far(0)
-    with scope("near2"):
-        near(2)
     with scope("mates0"):
         mates(0)
     with scope("comp0"):
         compute(0)
+    with scope("near2"):
+        near(2)
     with scope("far1"):
         far(1)
-    with scope("far2"):
-        far(2)
     with scope("mates1"):
         mates(1)
     with scope("comp1"):
         compute(1)
+    with scope("far2"):
+        far(2)
     with scope("mates2"):
         mates(2)
     with scope("qrel0"):
         ring_relay(qring[0])
     with scope("comp2"):
         compute(2)
-    border = remote(prod.at[pl.ds(ROWS, 8)], prod.at[pl.ds(0, 8)], bsem.at[0], bsem.at[1], dn)
-    border.start()
     with scope("own"):
         own_pair()
-    with scope("rel0"):
-        ring_relay(kring[0])
-        ring_relay(qring[1])
     with scope("conv"):
         border.wait_recv()
 
@@ -300,6 +298,10 @@
             tv[0:1] * prod[6:6 + ROWS, :] + tv[1:2] * prod[7:7 + ROWS, :] + tv[2:3] * prod[8:8 + ROWS, :]
         )
         conv[...] = (outer[...] * smoothed).astype(BF)
+    with scope("qrel1"):
+        ring_relay(qring[1])
+    with scope("rel0"):
+        ring_relay(kring[0])
     with scope("qrel2"):
         ring_relay(qring[2])
     with scope("rel1"):
@@ -524,8 +526,8 @@
     run(((send_stats, 1), (join_shares, 0)))
     last_keys(2, ((send_shares, 1), (merge, 0)))
     run((
-        (send_stats, 2), (join_shares, 1), (send_sums, 0), (send_shares, 2), (merge, 1),
-        (join_sums, 0), (send_sums, 1), (join_shares, 2), (merge, 2), (join_sums, 1),
+        (send_stats, 2), (join_shares, 1), (send_shares, 2), (send_sums, 0), (merge, 1),
+        (join_sums, 0), (join_shares, 2), (send_sums, 1), (merge, 2), (join_sums, 1),
         (send_sums, 2), (finish, 0), (row_lse, 0), (join_sums, 2), (finish, 1), (finish, 2),
     ))
     with scope("drain"):

time: 99.3 us -> 95.9 us (0.966)
  Pallas kernels: 95.3 us -> 92.1 us
    pallas_call x1, Pallas kernels: 95.3 us -> 92.1 us  [per_device(): pl.pallas_call(layer_kernel, out_shape=(jax.ShapeDtypeStruct((BLK, 2048),...]
where the time goes in v5:
time: 95.9 us; the launch traced here: 95.8 us
  Pallas kernels  92.1 us (96%)
  local copies, waits for them, and re-layouts  2.37 us (2%)
  between operations  1.3 us (1%)
    pallas_call x1, Pallas kernels, per_device(): pl.pallas_call(layer_kernel, out_shape=(jax.ShapeDtypeStruct((BLK, 2048),...  92.1 us
    unnamed x4, local copies, waits for them, and re-layouts  2.37 us

profile of v5, /device:TPU:97, one launch (start us, length us, event | category | flops | bytes accessed | tf_op | source)
XLA Modules:
  0.0 95.8 jit_solution(7315926889367453063)
XLA Ops:
  1.3 92.1 %layer.1 = (bf16[96,2048]{1,0:T(8,128)(2,1)}, f32[2,768]{1,0:T(2,128)}) custom-call(f32[16,128]{1,0:T(8,128)} %bitcast.5, f32[1]{0:T(128)S(6)} %copy.21.lam, f32[1,256]{1,0:T(1,128)} %bitcast.7, bf16[3,256]{1,0:T(4,128)(2,1)} %taps.1, f32[16,128]{1,0:T(8,128)} %constant.8.clone.oc, f32[16,128]{1,0:T(8,128)} %constant.9.clone.os_, ...), custom_call_target="tpu_custom_call" | custom-call | tf_op jit(solution)/shard_map/layer/pallas_call | solution.py:560
  93.4 0.0 copy-start
  93.4 1.8 %copy.22 = bf16[96,2048]{1,0:T(8,128)(2,1)} copy(bf16[96,2048]{1,0:T(8,128)(2,1)} %get-tuple-element.8) | data formatting | bytes 786432
  95.2 0.0 copy-done
  95.2 0.6 copy.23
Async XLA Ops:
  93.4 1.8 %copy-start = (f32[2,768]{1,0:T(2,128)S(1)}, f32[2,768]{1,0:T(2,128)}, u32[]{:S(2)}) copy-start(f32[2,768]{1,0:T(2,128)} %get-tuple-element.5) | copy-start | bytes 18436

commit v6 on v5

--- a/solution.py
+++ b/solution.py
@@ -524,9 +524,9 @@
     run(((send_stats, 0),))
     last_keys(1, ((send_shares, 0),))
     run(((send_stats, 1), (join_shares, 0)))
-    last_keys(2, ((send_shares, 1), (merge, 0)))
+    last_keys(2, ((send_shares, 1),))
     run((
-        (send_stats, 2), (join_shares, 1), (send_shares, 2), (send_sums, 0), (merge, 1),
+        (send_stats, 2), (join_shares, 1), (merge, 0), (send_shares, 2), (send_sums, 0), (merge, 1),
         (join_sums, 0), (join_shares, 2), (send_sums, 1), (merge, 2), (join_sums, 1),
         (send_sums, 2), (finish, 0), (row_lse, 0), (join_sums, 2), (finish, 1), (finish, 2),
     ))

time: 95.9 us -> 95 us (level)
  Pallas kernels: 92.1 us -> 91.1 us
where the time goes in v6:
time: 95 us; the launch traced here: 94.8 us
  Pallas kernels  91.1 us (96%)
  local copies, waits for them, and re-layouts  2.37 us (2%)
  between operations  1.3 us (1%)
    pallas_call x1, Pallas kernels, per_device(): pl.pallas_call(layer_kernel, out_shape=(jax.ShapeDtypeStruct((BLK, 2048),...  91.1 us
    unnamed x4, local copies, waits for them, and re-layouts  2.37 us

profile of v6, /device:TPU:97, one launch (start us, length us, event | category | flops | bytes accessed | tf_op | source)
XLA Modules:
  0.0 94.8 jit_solution(7242296658005744160)
XLA Ops:
  1.3 91.1 %layer.1 = (bf16[96,2048]{1,0:T(8,128)(2,1)}, f32[2,768]{1,0:T(2,128)}) custom-call(f32[16,128]{1,0:T(8,128)} %bitcast.5, f32[1]{0:T(128)S(6)} %copy.21.lam, f32[1,256]{1,0:T(1,128)} %bitcast.7, bf16[3,256]{1,0:T(4,128)(2,1)} %taps.1, f32[16,128]{1,0:T(8,128)} %constant.8.clone.oc, f32[16,128]{1,0:T(8,128)} %constant.9.clone.os_, ...), custom_call_target="tpu_custom_call" | custom-call | tf_op jit(solution)/shard_map/layer/pallas_call | solution.py:560
  92.4 0.0 copy-start
  92.4 1.8 %copy.22 = bf16[96,2048]{1,0:T(8,128)(2,1)} copy(bf16[96,2048]{1,0:T(8,128)(2,1)} %get-tuple-element.8) | data formatting | bytes 786432
  94.2 0.0 copy-done
  94.2 0.6 copy.23
Async XLA Ops:
  92.4 1.8 %copy-start = (f32[2,768]{1,0:T(2,128)S(1)}, f32[2,768]{1,0:T(2,128)}, u32[]{:S(2)}) copy-start(f32[2,768]{1,0:T(2,128)} %get-tuple-element.5) | copy-start | bytes 18436
